TPU v7x, 32 devices: a whole 2x2x4 slice. The times are simulated.
32 devices in a mesh: grp: 2 (over y), ep: 8 (over z, core), tp: 2 (over x).
Axes of the slice: x: 2, y: 2, z: 4, core: 2. Of those that a mesh axis runs over, the one named last changes fastest.
Arguments:
- recurrence_query_input: bfloat16 [2048, 2048], P(('grp', 'ep'), 'tp'), parts along dimension 0, may hold values from -6 to 6
- forget_gate_input: bfloat16 [2048, 2048], P(('grp', 'ep'), 'tp'), parts along dimension 0, may hold values from -6.5 to 6.5
- recurrence_value_input: bfloat16 [2048, 2048], P(('grp', 'ep'), 'tp'), parts along dimension 0, may hold values from -6 to 6
- output_gate_input: bfloat16 [2048, 2048], P(('grp', 'ep'), 'tp'), parts along dimension 0, may hold values from -6 to 6
- forget_lower_margin: float32 [2048], P('tp'), may hold values from 0 to 0.1
- position_decay_extra: float32 [2048, 16], P(('grp', 'ep'), 'tp'), parts along dimension 0, may hold values from -2.1 to 0
- head_norm_gain: float32 [2048], P('tp'), may hold values from 0.1 to 1.9
- recurrence_out_weight: bfloat16 [2048, 2048], P('tp'), may hold values from -0.125 to 0.125
- expert_hidden_state: bfloat16 [2048, 2048], P(('grp', 'ep')), parts along dimension 0, may hold values from -6 to 6
- chosen_expert_index: int32 [2048, 4], P(('grp', 'ep')), parts along dimension 0, may hold values from 0 to 7, all different within a row; in each aligned block of 128 rows (0 to 127, 128 to 255, ...) at most 128 rows name the same one
- chosen_expert_score: float32 [2048, 4], P(('grp', 'ep')), parts along dimension 0, may hold values from 0.02 to 1
- expert_norm_gain: float32 [2048], replicated, may hold values from 0.1 to 1.9
- routed_gate_weight: bfloat16 [8, 2048, 1024], P('ep', None, 'tp'), may hold values from -0.125 to 0.125
- routed_up_weight: bfloat16 [8, 2048, 1024], P('ep', None, 'tp'), may hold values from -0.125 to 0.125
- routed_down_weight: bfloat16 [8, 1024, 2048], P('ep', None, 'tp'), may hold values from -0.1875 to 0.1875
- shared_gate_weight: bfloat16 [2048, 1024], P(None, 'tp'), may hold values from -0.125 to 0.125
- shared_up_weight: bfloat16 [2048, 1024], P(None, 'tp'), may hold values from -0.125 to 0.125
- shared_down_weight: bfloat16 [1024, 2048], P(None, 'tp'), may hold values from -0.1875 to 0.1875
Outputs:
- recurrence_output: bfloat16 [2048, 2048], P(('grp', 'ep', 'tp')), parts along dimension 0
- expert_out: bfloat16 [2048, 2048], P(('grp', 'ep'), 'tp'), parts along dimension 0
There are 2 independent parts, one for each index of `grp`. A program takes and returns all parts, laid end to end along the dimension named above; an argument that names none is the same for every part. Nothing has to cross between parts.
Inputs may be any that keep to these rules, and one draw needn't show every extreme that they name: `chosen_expert_index`: each row names 4 different experts. In each aligned block of 128 rows (the rows of one index of ep) no expert is named by more than 128 rows, and in every draw some block names some expert exactly 128 times.
All inputs are finite; a program needn't handle non-finite values.
Results may differ from a plain program's by a relative error of at most 0.015.
Values may be sent and summed in bfloat16 or wider, within the bound.
A program may use at most 64 MiB of HBM per device.

v0:
```python
import functools

import jax
import jax.numpy as jnp
from jax import lax
from jax.experimental import pallas as pl
from jax.experimental.pallas import tpu as pltpu
from jax.sharding import PartitionSpec as P

HEAD_CHANNELS = 128
BLK = 64


EPSILON = 1e-06
ROUTED_SCALE = 2.5
PRECISION = lax.Precision.DEFAULT


DECAY_ROWS = 16


def carried_in(decay, state, axis):
    count, index = (lax.axis_size(axis), lax.axis_index(axis))
    depth = state.shape[1]
    rows = jnp.broadcast_to(decay[:, None, :], (decay.shape[0], DECAY_ROWS, decay.shape[1]))
    sent = jnp.concatenate([state, rows], axis=1).astype(jnp.bfloat16)
    everything = lax.all_gather(sent, axis)
    before = jnp.zeros_like(state)
    for k in range(count - 1):
        part = everything[k].astype(jnp.float32)
        new = part[:, depth : depth + 1] * before + part[:, :depth]
        before = jnp.where(k < index, new, before)
    return before


def mixer_half(
    recurrence_query_input,
    forget_gate_input,
    recurrence_value_input,
    output_gate_input,
    forget_lower_margin,
    position_decay_extra,
    head_norm_gain,
    recurrence_out_weight,
):
    length = recurrence_query_input.shape[0]
    head_tensor = position_decay_extra.shape[1]
    blocks = length // BLK
    queries = jax.nn.silu(recurrence_query_input.astype(jnp.float32))
    key_gate_value = forget_lower_margin[None, :] * jax.nn.sigmoid(
        -forget_gate_input.astype(jnp.float32)
    )
    decay_logarithm = jnp.log1p(-key_gate_value) + jnp.repeat(
        position_decay_extra, HEAD_CHANNELS, axis=1
    )
    value_rows = recurrence_value_input.astype(jnp.float32)

    def split_heads(tensor):
        return tensor.reshape(blocks, BLK, head_tensor, HEAD_CHANNELS).transpose(2, 0, 1, 3)

    query_heads = split_heads(queries)
    key_heads = split_heads(key_gate_value)
    value_heads = split_heads(value_rows)
    cum_decay = jnp.cumsum(split_heads(decay_logarithm), axis=2)
    middle = cum_decay[:, :, BLK // 2 - 1 : BLK // 2]
    block_end = cum_decay[:, :, BLK - 1 : BLK]
    scores = jnp.einsum(
        "hncd,hnsd->hncs",
        query_heads * jnp.exp(cum_decay - middle),
        key_heads * jnp.exp(middle - cum_decay),
        precision=PRECISION,
    )
    causal = jnp.tril(jnp.ones((BLK, BLK), dtype=bool))
    scores = jnp.where(causal, scores, 0.0)
    within = jnp.einsum("hncs,hnse->hnce", scores, value_heads, precision=PRECISION)
    updates = jnp.einsum(
        "hncd,hnce->nhed",
        key_heads * jnp.exp(block_end - cum_decay),
        value_heads,
        precision=PRECISION,
    )
    block_log = block_end[:, :, 0, :]
    block_decay = jnp.exp(block_log).transpose(1, 0, 2)

    state = jnp.zeros_like(updates[0])
    starts_list = []
    for block in range(blocks):
        starts_list.append(state)
        state = block_decay[block][:, None, :] * state + updates[block]
    local_final, local_starts = state, jnp.stack(starts_list)
    device_decay = jnp.exp(jnp.sum(block_log, axis=1))
    incoming = carried_in(device_decay, local_final, "ep")
    before = jnp.exp(jnp.cumsum(block_log, axis=1) - block_log).transpose(1, 0, 2)
    starts = local_starts + before[:, :, None, :] * incoming[None]
    carried = jnp.einsum(
        "hncd,nhed->hnce", query_heads * jnp.exp(cum_decay), starts, precision=PRECISION
    )
    outputs = (within + carried).transpose(1, 2, 0, 3).reshape(length, head_tensor, HEAD_CHANNELS)
    factor = lax.rsqrt(jnp.mean(outputs * outputs, axis=2, keepdims=True) + EPSILON)
    normed = (outputs * factor).reshape(length, head_tensor * HEAD_CHANNELS) * head_norm_gain[
        None, :
    ]
    gated_rows = (normed * jax.nn.silu(output_gate_input.astype(jnp.float32))).astype(jnp.bfloat16)
    partial = jnp.dot(
        gated_rows, recurrence_out_weight, preferred_element_type=jnp.float32
    ).astype(jnp.bfloat16)
    if lax.axis_size("tp") != 2:
        return lax.psum_scatter(partial, "tp", scatter_dimension=0, tiled=True)
    which, kept_rows = lax.axis_index("tp"), length // 2
    kept = lax.dynamic_slice_in_dim(partial, which * kept_rows, kept_rows)
    sent = lax.dynamic_slice_in_dim(partial, (1 - which) * kept_rows, kept_rows)
    received = lax.ppermute(sent, "tp", [(0, 1), (1, 0)])
    return (kept.astype(jnp.float32) + received.astype(jnp.float32)).astype(jnp.bfloat16)


def expert_half(
    expert_hidden_state,
    chosen_expert_index,
    chosen_expert_score,
    expert_norm_gain,
    routed_gate_weight,
    routed_up_weight,
    routed_down_weight,
    shared_gate_weight,
    shared_up_weight,
    shared_down_weight,
):
    tokens, top = chosen_expert_index.shape
    local_experts = routed_gate_weight.shape[0]
    devices = lax.axis_size("ep")
    experts = local_experts * devices
    capacity = min(tokens, 2 * tokens * top // experts)
    width_out = routed_down_weight.shape[2]
    features = expert_hidden_state.astype(jnp.float32)
    normed = (
        features
        * lax.rsqrt(jnp.mean(features * features, axis=1, keepdims=True) + EPSILON)
        * expert_norm_gain[None, :]
    ).astype(jnp.bfloat16)
    gates = ROUTED_SCALE * chosen_expert_score / jnp.sum(chosen_expert_score, axis=1, keepdims=True)
    flat_ids = chosen_expert_index.reshape(-1)
    onehot = (flat_ids[:, None] == jnp.arange(experts, dtype=jnp.int32)[None, :]).astype(jnp.int32)
    places = jnp.sum(onehot * (jnp.cumsum(onehot, axis=0) - 1), axis=1)
    slots = flat_ids * capacity + places
    owners = (
        jnp.full((experts * capacity,), tokens, jnp.int32)
        .at[slots]
        .set(jnp.arange(tokens * top, dtype=jnp.int32) // top)
    )
    padded = jnp.concatenate([normed, jnp.zeros((1, normed.shape[1]), jnp.bfloat16)], axis=0)
    outgoing = padded[owners].reshape(experts, capacity, normed.shape[1])
    piece = lax.all_to_all(outgoing, "ep", split_axis=0, concat_axis=0, tiled=True)
    grouped = piece.reshape(devices, local_experts, piece.shape[1], piece.shape[2])
    gate_part = jnp.einsum(
        "secd,edh->sech", grouped, routed_gate_weight, preferred_element_type=jnp.float32
    )
    up_part = jnp.einsum(
        "secd,edh->sech", grouped, routed_up_weight, preferred_element_type=jnp.float32
    )
    hidden = (jax.nn.silu(gate_part) * up_part).astype(jnp.bfloat16)
    hidden_rows = hidden.reshape(devices * local_experts, piece.shape[1], hidden.shape[3])
    flat_hidden = hidden_rows.reshape(experts * capacity, hidden_rows.shape[2])
    shared_hidden = (
        jax.nn.silu(jnp.dot(normed, shared_gate_weight, preferred_element_type=jnp.float32))
        * jnp.dot(normed, shared_up_weight, preferred_element_type=jnp.float32)
    ).astype(jnp.bfloat16)
    start_values = (
        jnp.zeros((experts * capacity, width_out), jnp.float32),
        jnp.zeros((tokens, width_out), jnp.float32),
    )
    routed_piece = lax.all_gather(flat_hidden, "tp", axis=1, tiled=True)
    shared_piece = lax.all_gather(shared_hidden, "tp", axis=1, tiled=True)
    count = routed_piece.shape[1]
    grouped = routed_piece.reshape(devices, local_experts, capacity, count)
    routed = jnp.einsum(
        "secn,enk->seck", grouped, routed_down_weight, preferred_element_type=jnp.float32
    )
    shared = jnp.dot(shared_piece, shared_down_weight, preferred_element_type=jnp.float32)
    routed_sum = routed.reshape(start_values[0].shape)
    answers = routed_sum.astype(jnp.bfloat16).reshape(experts, capacity, width_out)
    returned = lax.all_to_all(answers, "ep", split_axis=0, concat_axis=0, tiled=True)
    picked_rows = returned.reshape(experts * capacity, width_out)[slots].reshape(
        tokens, top, width_out
    )
    combined = shared + jnp.sum(gates[:, :, None] * picked_rows.astype(jnp.float32), axis=1)
    return combined.astype(jnp.bfloat16)


MESH = pl.DeviceIdType.MESH
LANES = 128


def expert_kernel(
    count,
    x_ref,
    gate_hbm,
    up_hbm,
    down_hbm,
    shared_gate_hbm,
    shared_up_hbm,
    shared_down_hbm,
    routed_ref,
    shared_ref,
    rows,
    gate_w,
    up_w,
    down_w,
    shared_gate_w,
    shared_up_w,
    shared_down_w,
    own_hidden,
    peer_hidden,
    load_sem,
    right_sem,
    left_sem,
    side_sem,
    row_sem,
    hidden_send,
    hidden_recv,
):
    chips = count // 2
    me = lax.axis_index("ep")
    half = lax.axis_index("tp")
    chip, core = me // 2, me % 2
    side = chip * 2 + 1 - core
    partner = 1 - half
    block_rows = x_ref.shape[0]
    width = gate_w.shape[0]
    units = gate_w.shape[1]
    has_right, has_left = chip < chips - 1, chip > 0

    def half_rows(ref, which):
        return ref.at[pl.ds(pl.multiple_of(which * units, units), units), :]

    loads = [
        (shared_gate_hbm, shared_gate_w),
        (shared_up_hbm, shared_up_w),
        (gate_hbm.at[0], gate_w),
        (up_hbm.at[0], up_w),
        (half_rows(down_hbm.at[0], half), down_w.at[0]),
        (half_rows(down_hbm.at[0], partner), down_w.at[1]),
        (half_rows(shared_down_hbm, half), shared_down_w.at[0]),
        (half_rows(shared_down_hbm, partner), shared_down_w.at[1]),
        (x_ref, rows.at[me]),
    ]
    copies = [
        pltpu.make_async_copy(source, target, load_sem.at[i])
        for i, (source, target) in enumerate(loads)
    ]
    for copy in copies:
        copy.start()

    barrier = pltpu.get_barrier_semaphore()
    pl.semaphore_signal(barrier, inc=1, device_id={"ep": side}, device_id_type=MESH)
    pl.semaphore_signal(barrier, inc=1, device_id={"tp": partner}, device_id_type=MESH)

    @pl.when(has_right)
    def _():
        pl.semaphore_signal(barrier, inc=1, device_id={"ep": me + 2}, device_id_type=MESH)

    @pl.when(has_left)
    def _():
        pl.semaphore_signal(barrier, inc=1, device_id={"ep": me - 2}, device_id_type=MESH)

    pl.semaphore_wait(barrier, 2 + has_right.astype(jnp.int32) + has_left.astype(jnp.int32))

    def row_copy(source, block, sems, target):
        return pltpu.make_async_remote_copy(
            src_ref=source,
            dst_ref=rows.at[block],
            send_sem=sems.at[block],
            recv_sem=row_sem.at[block],
            device_id={"ep": target},
            device_id_type=MESH,
        )

    def hidden_copy(step):
        return pltpu.make_async_remote_copy(
            src_ref=own_hidden.at[step],
            dst_ref=peer_hidden.at[step],
            send_sem=hidden_send.at[step],
            recv_sem=hidden_recv.at[step],
            device_id={"tp": partner},
            device_id_type=MESH,
        )

    def block_of(step):
        k, odd = step // 2, step % 2
        inner = jnp.minimum(chip, chips - 1 - chip)
        near = jnp.where(k % 2 == 1, chip - (k + 1) // 2, chip + k // 2)
        far = jnp.where(chip <= chips - 1 - chip, k, chips - 1 - k)
        source = jnp.where(k <= 2 * inner, near, far)
        return source, source * 2 + jnp.where(odd == 1, 1 - core, core)

    def goes_right(source):
        return jnp.logical_and(source <= chip, has_right)

    def goes_left(source):
        return jnp.logical_and(source >= chip, has_left)

    @pl.when(has_right)
    def _():
        row_copy(x_ref, me, right_sem, me + 2).start()

    @pl.when(has_left)
    def _():
        row_copy(x_ref, me, left_sem, me - 2).start()

    row_copy(x_ref, me, side_sem, side).start()

    copies[0].wait()
    copies[1].wait()
    gate_part = jnp.dot(
        x_ref[:, :width], shared_gate_w[...], preferred_element_type=jnp.float32
    )
    up_part = jnp.dot(x_ref[:, :width], shared_up_w[...], preferred_element_type=jnp.float32)
    own_hidden[count] = (jax.nn.silu(gate_part) * up_part).astype(jnp.bfloat16)
    for copy in copies[2:]:
        copy.wait()

    def down(step, weight):
        hidden_copy(step).wait_recv()
        return jnp.dot(
            own_hidden[step], weight[0], preferred_element_type=jnp.float32
        ) + jnp.dot(peer_hidden[step], weight[1], preferred_element_type=jnp.float32)

    def routed_down(step):
        _, block = block_of(step)
        place = pl.ds(pl.multiple_of(block * block_rows, block_rows), block_rows)
        routed_ref[place, :] = down(step, down_w).astype(jnp.bfloat16)

    def turn(step, _):
        source, block = block_of(step)
        odd = step % 2

        @pl.when(step > 0)
        def _():
            row_copy(x_ref, block, side_sem, side).wait_recv()

        @pl.when(jnp.logical_and(step > 0, odd == 0))
        def _():
            @pl.when(goes_right(source))
            def _():
                row_copy(rows.at[block], block, right_sem, me + 2).start()

            @pl.when(goes_left(source))
            def _():
                row_copy(rows.at[block], block, left_sem, me - 2).start()

            row_copy(rows.at[block], block, side_sem, side).start()

        x = rows[block, :, :width]
        tail = rows[block, :, width:].astype(jnp.float32)
        lane = lax.broadcasted_iota(jnp.int32, tail.shape, 1)
        own_gate = jnp.sum(
            jnp.where(lane % (LANES // 2) == me, tail, 0.0), axis=1, keepdims=True
        )
        gate_part = jnp.dot(x, gate_w[...], preferred_element_type=jnp.float32)
        up_part = jnp.dot(x, up_w[...], preferred_element_type=jnp.float32)
        own_hidden[step] = (jax.nn.silu(gate_part) * up_part * own_gate).astype(jnp.bfloat16)

        @pl.when(step == 0)
        def _():
            hidden_copy(count).start()

        @pl.when(step > 0)
        def _():
            routed_down(step - 1)

        hidden_copy(step).start()
        return 0

    lax.fori_loop(0, count, turn, 0)
    shared_ref[...] = down(count, shared_down_w)
    routed_down(count - 1)

    def finish(step, _):
        source, block = block_of(step)
        hidden_copy(step).wait_send()

        @pl.when(step % 2 == 0)
        def _():
            @pl.when(goes_right(source))
            def _():
                row_copy(x_ref, block, right_sem, me + 2).wait_send()

            @pl.when(goes_left(source))
            def _():
                row_copy(x_ref, block, left_sem, me - 2).wait_send()

            row_copy(x_ref, block, side_sem, side).wait_send()

        return 0

    lax.fori_loop(0, count, finish, 0)
    hidden_copy(count).wait_send()


def dense_expert_half(
    expert_hidden_state,
    chosen_expert_index,
    chosen_expert_score,
    expert_norm_gain,
    routed_gate_weight,
    routed_up_weight,
    routed_down_weight,
    shared_gate_weight,
    shared_up_weight,
    shared_down_weight,
):
    tokens = chosen_expert_index.shape[0]
    count = lax.axis_size("ep")
    features = expert_hidden_state.astype(jnp.float32)
    width = features.shape[1]
    units, width_out = routed_gate_weight.shape[2], routed_down_weight.shape[2]
    normed = (
        features
        * lax.rsqrt(jnp.mean(features * features, axis=1, keepdims=True) + EPSILON)
        * expert_norm_gain[None, :]
    ).astype(jnp.bfloat16)
    gates = ROUTED_SCALE * chosen_expert_score / jnp.sum(chosen_expert_score, axis=1, keepdims=True)
    slots = LANES // 2
    chosen = chosen_expert_index[:, :, None] == jnp.arange(slots, dtype=jnp.int32)[None, None, :]
    gate_table = jnp.sum(jnp.where(chosen, gates[:, :, None], 0.0), axis=1)
    high = gate_table.astype(jnp.bfloat16)
    low = (gate_table - high.astype(jnp.float32)).astype(jnp.bfloat16)
    sent = jnp.concatenate([normed, high, low], axis=1)
    hbm = pl.BlockSpec(memory_space=pl.ANY)
    vmem = pl.BlockSpec(memory_space=pltpu.VMEM)
    weight = pltpu.VMEM((width, units), jnp.bfloat16)
    down_weight = pltpu.VMEM((2, units, width_out), jnp.bfloat16)
    hidden = pltpu.VMEM((count + 1, tokens, units), jnp.bfloat16)
    block_sems = pltpu.SemaphoreType.DMA((count,))
    routed, shared = pl.pallas_call(
        functools.partial(expert_kernel, count),
        out_shape=(
            jax.ShapeDtypeStruct((count * tokens, width_out), jnp.bfloat16),
            jax.ShapeDtypeStruct((tokens, width_out), jnp.float32),
        ),
        in_specs=[vmem] + [hbm] * 6,
        out_specs=(vmem, vmem),
        scratch_shapes=[
            pltpu.VMEM((count, tokens, width + LANES), jnp.bfloat16),
            weight,
            weight,
            down_weight,
            weight,
            weight,
            down_weight,
            hidden,
            hidden,
            pltpu.SemaphoreType.DMA((9,)),
            block_sems,
            block_sems,
            block_sems,
            block_sems,
            pltpu.SemaphoreType.DMA((count + 1,)),
            pltpu.SemaphoreType.DMA((count + 1,)),
        ],
        compiler_params=pltpu.CompilerParams(
            collective_id=0, has_side_effects=True, vmem_limit_bytes=48 * 1024 * 1024
        ),
        cost_estimate=pl.CostEstimate(
            flops=45_000_000_000, bytes_accessed=16_000_000, transcendentals=0
        ),
        name="expert_kernel",
    )(
        sent,
        routed_gate_weight,
        routed_up_weight,
        routed_down_weight,
        shared_gate_weight,
        shared_up_weight,
        shared_down_weight,
    )
    total = lax.psum_scatter(routed, "ep", scatter_dimension=0, tiled=True)
    return (shared + total.astype(jnp.float32)).astype(jnp.bfloat16)


def per_device(
    recurrence_query_input,
    forget_gate_input,
    recurrence_value_input,
    output_gate_input,
    forget_lower_margin,
    position_decay_extra,
    head_norm_gain,
    recurrence_out_weight,
    expert_hidden_state,
    chosen_expert_index,
    chosen_expert_score,
    expert_norm_gain,
    routed_gate_weight,
    routed_up_weight,
    routed_down_weight,
    shared_gate_weight,
    shared_up_weight,
    shared_down_weight,
):
    recurrence_output = mixer_half(
        recurrence_query_input,
        forget_gate_input,
        recurrence_value_input,
        output_gate_input,
        forget_lower_margin,
        position_decay_extra,
        head_norm_gain,
        recurrence_out_weight,
    )
    tokens, top = chosen_expert_index.shape
    experts = routed_gate_weight.shape[0] * lax.axis_size("ep")
    every_row_fits = 2 * top >= experts and routed_gate_weight.shape[0] == 1 and experts <= 64
    half = dense_expert_half if every_row_fits else expert_half
    expert_out = half(
        expert_hidden_state,
        chosen_expert_index,
        chosen_expert_score,
        expert_norm_gain,
        routed_gate_weight,
        routed_up_weight,
        routed_down_weight,
        shared_gate_weight,
        shared_up_weight,
        shared_down_weight,
    )
    return (recurrence_output, expert_out)


def solution(mesh):
    in_specs = (
        P(("grp", "ep"), "tp"),
        P(("grp", "ep"), "tp"),
        P(("grp", "ep"), "tp"),
        P(("grp", "ep"), "tp"),
        P("tp"),
        P(("grp", "ep"), "tp"),
        P("tp"),
        P("tp", None),
        P(("grp", "ep"), None),
        P(("grp", "ep"), None),
        P(("grp", "ep"), None),
        P(),
        P("ep", None, "tp"),
        P("ep", None, "tp"),
        P("ep", None, "tp"),
        P(None, "tp"),
        P(None, "tp"),
        P(None, "tp"),
    )
    out_specs = (P(("grp", "ep", "tp"), None), P(("grp", "ep"), "tp"))
    return jax.shard_map(
        per_device, mesh=mesh, in_specs=in_specs, out_specs=out_specs, check_vma=False
    )
```

profile of v0, /device:TPU:0, one launch (start us, length us, event | category | flops | bytes accessed | tf_op | source)
XLA Modules:
  0.0 135.9 jit_solution(18066084793452295340)
XLA Ops:
  7.2 0.8 copy.72
  8.0 0.2 broadcast_in_dim.23
  8.2 1.3 fusion.51
  9.5 0.1 copy.91
  9.6 0.2 fusion.26
  9.9 0.1 fusion.11
  10.0 0.1 copy.89
  10.2 0.4 copy-done.8
  10.7 1.1 bitcast_multiply_fusion.1
  11.8 0.4 convolution_bitcast_fusion
  12.2 0.9 fusion.25
  13.1 0.7 pad_maximum_fusion
  14.1 0.2 fusion.4
  14.3 0.1 copy.86
  14.4 0.2 fusion.6
  14.6 0.6 subtract_convert_fusion
  15.2 0.9 concatenate.15.x_ref
  16.2 75.2 %expert_kernel.1 = (bf16[1024,1024]{1,0:T(8,128)(2,1)}, f32[128,1024]{1,0:T(8,128)S(1)}) custom-call(bf16[128,2176]{1,0:T(8,128)(2,1)S(1)} %concatenate.15.x_ref, bf16[1,2048,512]{2,1,0:T(8,128)(2,1)S(1)} %copy-done, bf16[1,2048,512]{2,1,0:T(8,128)(2,1)} %up_hbm.1, bf16[1,1024,1024]{2,1,0:T(8,128)(2,1)} %down_hbm.1, bf16[2048,512]{1,0:T(8,128)(2,1)} %shared_gate_hbm.1, ...), custom_call_target="tpu_custom_call" | custom-call | flops 44999999488 | bytes 16000000 | tf_op jit(solution)/shard_map/expert_kernel/pallas_call | solution.py:434
  91.5 0.8 fusion.3
  92.4 0.1 copy-done.7
  92.5 0.4 fusion.1
  92.9 1.8 %fusion.36 = (f32[8,144,128]{2,1,0:T(8,128)S(1)}, f32[8,144,128]{2,1,0:T(8,128)S(1)}, f32[8,144,128]{2,1,0:T(8,128)S(1)}, f32[8,144,128]{2,1,0:T(8,128)S(1)}, f3...) fusion(bf16[8,8,144,128]{3,2,1,0:T(8,128)(2,1)} %all-gather.2.cloned.1.call-done), kind=kLoop, calls=%fused_computation.66 | loop fusion | flops 1032192 | bytes 6193152 | tf_op jit(solution)/shard_map/convert_element_type | solution.py:30
  94.9 0.4 fusion.18
  95.3 0.6 copy-done.3
  96.0 0.6 multiply_reduce_fusion
  96.7 0.3 copy.82
  97.0 0.2 mul.230
  97.2 3.1 %convolution_convert_fusion = bf16[128,2048]{1,0:T(8,128)(2,1)S(1)} fusion(bf16[1024,2048]{1,0:T(8,128)(2,1)} %param.25, bf16[128,1024]{1,0:T(8,128)(2,1)S(1)} %copy-done.12, f32[16,8,8,128]{3,2,1,0:T(8,128)S(1)} %bitcast.136, f32[16,8,8,128]{3,2,1,0:T(8,128)S(1)} %bitcast.137, f32[1024]{0:T(1024)S(1)} %copy-done.13), kind=kOutput, calls=%fused_computation | convolution fusion | flops 538312704 | bytes 6033408 | tf_op jit(solution)/shard_map/dot_general | solution.py:104
  100.3 2.3 %collective-permute-start = (bf16[64,2048]{1,0:T(8,128)(2,1)S(1)}, bf16[64,2048]{1,0:T(8,128)(2,1)S(1)}, u32[]{:S(2)}, u32[]{:S(2)}) collective-permute-start(bf16[64,2048]{1,0:T(8,128)(2,1)S(1)} %constant_dynamic-slice_fusion), channel_id=1, source_target_pairs={{0,1},{1,0},{2,3},{3,2},{4,5},{5,4},{6,7},{7,6},{8,9},{9,8},{10,11... | collective-permute-start | bytes 786440 | tf_op jit(solution)/shard_map/ppermute | solution.py:112
  102.6 23.9 %reduce-scatter.2.cloned.1.call-done = bf16[128,1024]{1,0:T(8,128)(2,1)} async-done(((bf16[1024,1024]{1,0:T(8,128)(2,1)}), bf16[128,1024]{1,0:T(8,128)(2,1)}) %reduce-scatter.2.cloned.1.call-update) | async-done | bytes 262160 | tf_op jit(solution)/shard_map/reduce_scatter | solution.py:476
  126.6 1.7 %add_convert_fusion = bf16[128,1024]{1,0:T(8,128)(2,1)} fusion(f32[128,1024]{1,0:T(8,128)S(1)} %get-tuple-element.4, bf16[128,1024]{1,0:T(8,128)(2,1)} %reduce-scatter.2.cloned.1.call-done), kind=kLoop, calls=%fused_computation.60 | loop fusion | flops 393216 | bytes 1048576 | tf_op jit(solution)/shard_map/convert_element_type | solution.py:477
  128.3 0.8 add_convert_fusion.1
  (56 shorter events, 0.8 us)
Async XLA Ops:
  7.2 85.7 %all-gather.2.cloned.1.call-start = ((), (), s32[]{:S(2)}) async-start(), calls=%async_computation.1 | async-start | bytes 2654208 | tf_op jit(solution)/shard_map/all_gather | solution.py:27
  8.2 1.7 %copy-start.5 = (bf16[128,1024]{1,0:T(8,128)(2,1)S(1)}, bf16[128,1024]{1,0:T(8,128)(2,1)}, u32[]{:S(2)}) copy-start(bf16[128,1024]{1,0:T(8,128)(2,1)} %param.18) | copy-start | bytes 786436
  9.6 1.0 copy-start.8
  9.8 2.0 %copy-start.1 = (f32[8,2,64,128]{3,0,1,2:T(8,128)}, f32[8,2,64,128]{3,0,1,2:T(8,128)S(1)}, u32[]{:S(2)}) copy-start(f32[8,2,64,128]{3,0,1,2:T(8,128)S(1)} %fusion.26) | copy-start | bytes 1572868
  11.8 2.1 %copy-start.10 = (f32[128,4]{0,1:T(4,128)S(1)}, f32[128,4]{0,1:T(4,128)}, u32[]{:S(2)}) copy-start(f32[128,4]{0,1:T(4,128)} %param.28) | copy-start | bytes 6148
  11.8 2.1 %copy-start.11 = (s32[128,4]{0,1:T(4,128)S(1)}, s32[128,4]{0,1:T(4,128)}, u32[]{:S(2)}) copy-start(s32[128,4]{0,1:T(4,128)} %param.27) | copy-start | bytes 6148
  11.8 2.3 %copy-start.2 = (bf16[128,2048]{1,0:T(8,128)(2,1)S(1)}, bf16[128,2048]{1,0:T(8,128)(2,1)}, u32[]{:S(2)}) copy-start(bf16[128,2048]{1,0:T(8,128)(2,1)} %param.26) | copy-start | bytes 1572868
  12.1 2.2 %copy-start.9 = (f32[2048]{0:T(1024)S(1)}, f32[2048]{0:T(1024)}, u32[]{:S(2)}) copy-start(f32[2048]{0:T(1024)} %param.29) | copy-start | bytes 24580
  13.1 3.1 %copy-start = (bf16[1,2048,512]{2,1,0:T(8,128)(2,1)S(1)}, bf16[1,2048,512]{2,1,0:T(8,128)(2,1)}, u32[]{:S(2)}) copy-start(bf16[1,2048,512]{2,1,0:T(8,128)(2,1)} %gate_hbm.1) | copy-start | bytes 6291460
  13.8 112.8 %reduce-scatter.2.cloned.1.call-start = ((), (), s32[]{:S(2)}) async-start(), calls=%async_computation.2 | async-start | bytes 2359296 | tf_op jit(solution)/shard_map/reduce_scatter | solution.py:476
  91.4 1.0 copy-start.6
  91.4 1.1 copy-start.7
  94.8 1.0 copy-start.3
  94.9 1.1 copy-start.4
  95.3 1.9 %copy-start.12 = (bf16[128,1024]{1,0:T(8,128)(2,1)S(1)}, bf16[128,1024]{1,0:T(8,128)(2,1)}, u32[]{:S(2)}) copy-start(bf16[128,1024]{1,0:T(8,128)(2,1)} %param.21) | copy-start | bytes 786436
  95.3 1.9 %copy-start.13 = (f32[1024]{0:T(1024)S(1)}, f32[1024]{0:T(1024)}, u32[]{:S(2)}) copy-start(f32[1024]{0:T(1024)} %param.24) | copy-start | bytes 12292
  100.3 28.0 %collective-permute-start = (bf16[64,2048]{1,0:T(8,128)(2,1)S(1)}, bf16[64,2048]{1,0:T(8,128)(2,1)S(1)}, u32[]{:S(2)}, u32[]{:S(2)}) collective-permute-start(bf16[64,2048]{1,0:T(8,128)(2,1)S(1)} %constant_dynamic-slice_fusion), channel_id=1, source_target_pairs={{0,1},{1,0},{2,3},{3,2},{4,5},{5,4},{6,7},{7,6},{8,9},{9,8},{10,11... | collective-permute-start | bytes 786440 | tf_op jit(solution)/shard_map/ppermute | solution.py:112
Sparse Core Ops, SparseCore 0:
  13.9 42.2 all-gather.1
  91.6 34.9 reduce-scatter.1
where the time goes:
time: 136 us
  Pallas kernels  75.2 us (55%)
  waiting for transfers between devices  24 us (18%)
  between operations  14.5 us (11%)
  other arithmetic  11 us (8%)
  matrix products  4.39 us (3%)
  local copies, waits for them, and re-layouts  4.37 us (3%)
  starting transfers between devices  2.41 us (2%)
    pallas_call x1, Pallas kernels, dense_expert_half(): pl.pallas_call(functools.partial(expert_kernel, count), out_shape=(jax.Sh...  75.2 us
    reduce_scatter x1, waiting for transfers between devices, dense_expert_half(): total = lax.psum_scatter(routed, 'ep', scatter_dimension=0, tiled=True)  23.9 us
    dot_general x1, matrix products, mixer_half(): jnp.dot(gated_rows, recurrence_out_weight, preferred_element_type=jnp.flo...  3.08 us
  transfers between devices with their start and end apart: 3, of which 1 were waited for; matrix products, arithmetic and copies ran while one was open for 9% of the time, Pallas kernels for 55%

commit v1 on v0

--- a/solution.py
+++ b/solution.py
@@ -188,60 +188,190 @@
 
 MESH = pl.DeviceIdType.MESH
 LANES = 128
-
-
-def expert_kernel(
+SPLIT = 2
+KINDS = ("NO", "SR", "SL", "RF", "MA", "ST", "H", "D", "S", "FIN", "MB", "MO")
+NUMBER = {name: place for place, name in enumerate(KINDS)}
+
+
+ORDERS = (
+    (
+        ("SR", 0, 0), ("SR", 0, 1), ("MA", 0, 0), ("H", 4, 0), ("H", 0, 0), ("ST", 0, 0),
+        ("H", 0, 1), ("MB", 0, 0), ("RF", 1, 0), ("D", 4, 0), ("D", 0, 0), ("H", 1, 0),
+        ("RF", 1, 1), ("D", 0, 1), ("H", 1, 1), ("RF", 2, 0), ("MO", 0, 0), ("H", 2, 0),
+        ("D", 1, 0), ("RF", 2, 1), ("S", 1, 0), ("D", 1, 1), ("H", 2, 1), ("S", 1, 1),
+        ("D", 2, 0), ("RF", 3, 0), ("S", 2, 0), ("H", 3, 0), ("D", 2, 1), ("S", 2, 1),
+        ("RF", 3, 1), ("H", 3, 1), ("D", 3, 0), ("S", 3, 0), ("D", 3, 1), ("S", 3, 1),
+        ("FIN", 0, 0), ("FIN", 0, 1),
+    ),
+    (
+        ("SL", 1, 0), ("SR", 1, 0), ("SL", 1, 1), ("SR", 1, 1), ("MA", 0, 0), ("H", 4, 0),
+        ("H", 1, 0), ("H", 1, 1), ("RF", 0, 0), ("RF", 2, 0), ("D", 4, 0), ("H", 0, 0),
+        ("H", 2, 0), ("D", 1, 0), ("RF", 0, 1), ("RF", 2, 1), ("D", 1, 1), ("H", 0, 1),
+        ("ST", 0, 0), ("H", 2, 1), ("D", 0, 0), ("RF", 3, 0), ("MB", 0, 0), ("D", 2, 0),
+        ("H", 3, 0), ("D", 0, 1), ("RF", 3, 1), ("D", 2, 1), ("H", 3, 1), ("MO", 0, 0),
+        ("D", 3, 0), ("S", 2, 0), ("D", 3, 1), ("FIN", 1, 0), ("S", 2, 1), ("FIN", 1, 1),
+        ("S", 3, 0), ("S", 3, 1), ("S", 0, 0), ("S", 0, 1),
+    ),
+    (
+        ("SR", 2, 0), ("SL", 2, 0), ("SR", 2, 1), ("SL", 2, 1), ("MA", 0, 0), ("H", 4, 0),
+        ("H", 2, 0), ("H", 2, 1), ("RF", 3, 0), ("RF", 1, 0), ("D", 4, 0), ("H", 3, 0),
+        ("H", 1, 0), ("D", 2, 0), ("RF", 3, 1), ("RF", 1, 1), ("D", 2, 1), ("H", 3, 1),
+        ("H", 1, 1), ("D", 3, 0), ("RF", 0, 0), ("D", 1, 0), ("H", 0, 0), ("D", 3, 1),
+        ("RF", 0, 1), ("D", 1, 1), ("H", 0, 1), ("ST", 0, 0), ("D", 0, 0), ("MB", 0, 0),
+        ("D", 0, 1), ("S", 1, 0), ("MO", 0, 0), ("S", 1, 1), ("FIN", 2, 0), ("FIN", 2, 1),
+        ("S", 0, 0), ("S", 3, 0), ("S", 0, 1), ("S", 3, 1),
+    ),
+    (
+        ("SL", 3, 0), ("SL", 3, 1), ("MA", 0, 0), ("H", 4, 0), ("H", 3, 0), ("H", 3, 1),
+        ("RF", 2, 0), ("D", 4, 0), ("H", 2, 0), ("D", 3, 0), ("RF", 2, 1), ("D", 3, 1),
+        ("H", 2, 1), ("D", 2, 0), ("RF", 1, 0), ("S", 2, 0), ("H", 1, 0), ("D", 2, 1),
+        ("S", 2, 1), ("RF", 1, 1), ("H", 1, 1), ("D", 1, 0), ("S", 1, 0), ("RF", 0, 0),
+        ("H", 0, 0), ("D", 1, 1), ("S", 1, 1), ("RF", 0, 1), ("H", 0, 1), ("ST", 0, 0),
+        ("D", 0, 0), ("MB", 0, 0), ("S", 0, 0), ("D", 0, 1), ("S", 0, 1), ("MO", 0, 0),
+        ("FIN", 3, 0), ("FIN", 3, 1),
+    ),
+)
+
+
+def chip_orders(chips):
+    return ORDERS
+
+
+def packed_orders(chips):
+    orders = chip_orders(chips)
+    steps = max(len(order) for order in orders)
+    steps = -(-steps // 3) * 3
+    words = []
+    for order in orders:
+        codes = [NUMBER[kind] * 16 + source * SPLIT + part for kind, source, part in order]
+        codes = codes + [0] * (steps - len(codes))
+        words.append(
+            [codes[i] + 256 * codes[i + 1] + 65536 * codes[i + 2] for i in range(0, steps, 3)]
+        )
+    return steps, words
+
+
+def dot(a, b):
+    return jnp.dot(a, b, preferred_element_type=jnp.float32)
+
+
+def dot_nt(a, b):
+    return lax.dot_general(a, b, (((1,), (1,)), ((), ())), preferred_element_type=jnp.float32)
+
+
+def dot_tn(a, b):
+    return lax.dot_general(a, b, (((0,), (0,)), ((), ())), preferred_element_type=jnp.float32)
+
+
+def fused_kernel(
     count,
-    x_ref,
+    query_hbm,
+    forget_hbm,
+    value_hbm,
+    output_gate_hbm,
+    out_weight_hbm,
+    x_hbm,
     gate_hbm,
     up_hbm,
     down_hbm,
     shared_gate_hbm,
     shared_up_hbm,
     shared_down_hbm,
-    routed_ref,
-    shared_ref,
-    rows,
+    margin_ref,
+    extra_ref,
+    head_gain_ref,
+    index_ref,
+    score_ref,
+    gain_ref,
+    recurrent_ref,
+    expert_ref,
+    query_v,
+    forget_v,
+    value_v,
+    output_gate_v,
+    out_weight_v,
+    x_v,
     gate_w,
     up_w,
     down_w,
-    shared_gate_w,
-    shared_up_w,
-    shared_down_w,
+    rows,
+    gates,
     own_hidden,
     peer_hidden,
+    result,
+    side_result,
+    inward,
+    inward_left,
+    inward_right,
+    outward,
+    local_out,
+    carried_query,
+    own_state,
+    own_decay,
+    side_state,
+    side_decay,
+    before,
+    next_state,
+    gated,
+    mixed,
+    mixed_peer,
     load_sem,
+    row_sem,
+    table_sem,
     right_sem,
     left_sem,
     side_sem,
-    row_sem,
+    table_right,
+    table_left,
+    table_side,
     hidden_send,
     hidden_recv,
+    result_send,
+    result_recv,
+    outward_send,
+    inward_recv,
+    left_recv,
+    right_recv,
+    state_send,
+    state_recv,
+    mixed_send,
+    mixed_recv,
 ):
+    f32, bf16 = jnp.float32, jnp.bfloat16
     chips = count // 2
     me = lax.axis_index("ep")
     half = lax.axis_index("tp")
     chip, core = me // 2, me % 2
-    side = chip * 2 + 1 - core
+    other = 1 - core
+    side = chip * 2 + other
     partner = 1 - half
-    block_rows = x_ref.shape[0]
-    width = gate_w.shape[0]
-    units = gate_w.shape[1]
     has_right, has_left = chip < chips - 1, chip > 0
+    length = query_v.shape[0]
+    heads = extra_ref.shape[1]
+    mine = heads // 2
+    part_rows = rows.shape[1]
+    units = gate_w.shape[2]
+    routed = chips * SPLIT
+    steps, words = packed_orders(chips)
 
     def half_rows(ref, which):
         return ref.at[pl.ds(pl.multiple_of(which * units, units), units), :]
 
     loads = [
-        (shared_gate_hbm, shared_gate_w),
-        (shared_up_hbm, shared_up_w),
-        (gate_hbm.at[0], gate_w),
-        (up_hbm.at[0], up_w),
-        (half_rows(down_hbm.at[0], half), down_w.at[0]),
-        (half_rows(down_hbm.at[0], partner), down_w.at[1]),
-        (half_rows(shared_down_hbm, half), shared_down_w.at[0]),
-        (half_rows(shared_down_hbm, partner), shared_down_w.at[1]),
-        (x_ref, rows.at[me]),
+        (x_hbm, x_v),
+        (forget_hbm, forget_v),
+        (query_hbm, query_v),
+        (value_hbm, value_v),
+        (shared_gate_hbm, gate_w.at[1]),
+        (shared_up_hbm, up_w.at[1]),
+        (gate_hbm.at[0], gate_w.at[0]),
+        (up_hbm.at[0], up_w.at[0]),
+        (half_rows(shared_down_hbm, half), down_w.at[1, 0]),
+        (half_rows(shared_down_hbm, partner), down_w.at[1, 1]),
+        (half_rows(down_hbm.at[0], half), down_w.at[0, 0]),
+        (half_rows(down_hbm.at[0], partner), down_w.at[0, 1]),
+        (output_gate_hbm, output_gate_v),
+        (out_weight_hbm, out_weight_v),
     ]
     copies = [
         pltpu.make_async_copy(source, target, load_sem.at[i])
@@ -262,141 +392,481 @@
     def _():
         pl.semaphore_signal(barrier, inc=1, device_id={"ep": me - 2}, device_id_type=MESH)
 
-    pl.semaphore_wait(barrier, 2 + has_right.astype(jnp.int32) + has_left.astype(jnp.int32))
-
-    def row_copy(source, block, sems, target):
+    def remote(source, target, send, recv, **device):
         return pltpu.make_async_remote_copy(
             src_ref=source,
-            dst_ref=rows.at[block],
-            send_sem=sems.at[block],
-            recv_sem=row_sem.at[block],
-            device_id={"ep": target},
+            dst_ref=target,
+            send_sem=send,
+            recv_sem=recv,
+            device_id=device,
             device_id_type=MESH,
         )
 
-    def hidden_copy(step):
-        return pltpu.make_async_remote_copy(
-            src_ref=own_hidden.at[step],
-            dst_ref=peer_hidden.at[step],
-            send_sem=hidden_send.at[step],
-            recv_sem=hidden_recv.at[step],
-            device_id={"tp": partner},
-            device_id_type=MESH,
+    def row_copy(arg, sems, target):
+        block = arg * 2 + core
+        return remote(rows.at[block], rows.at[block], sems.at[arg], row_sem.at[block], ep=target)
+
+    def table_copy(source, sems, target):
+        block = source * 2 + core
+        return remote(
+            gates.at[block], gates.at[block], sems.at[source], table_sem.at[block], ep=target
         )
 
-    def block_of(step):
-        k, odd = step // 2, step % 2
-        inner = jnp.minimum(chip, chips - 1 - chip)
-        near = jnp.where(k % 2 == 1, chip - (k + 1) // 2, chip + k // 2)
-        far = jnp.where(chip <= chips - 1 - chip, k, chips - 1 - k)
-        source = jnp.where(k <= 2 * inner, near, far)
-        return source, source * 2 + jnp.where(odd == 1, 1 - core, core)
-
-    def goes_right(source):
-        return jnp.logical_and(source <= chip, has_right)
-
-    def goes_left(source):
-        return jnp.logical_and(source >= chip, has_left)
+    def arrived_row(block):
+        remote(rows.at[block], rows.at[block], side_sem.at[0], row_sem.at[block], ep=side).wait_recv()
+
+    def arrived_table(block):
+        remote(
+            gates.at[block], gates.at[block], table_side.at[0], table_sem.at[block], ep=side
+        ).wait_recv()
+
+    def hidden_copy(arg):
+        return remote(
+            own_hidden.at[arg],
+            peer_hidden.at[arg],
+            hidden_send.at[arg],
+            hidden_recv.at[arg],
+            tp=partner,
+        )
+
+    def result_copy(arg):
+        return remote(
+            result.at[arg, other],
+            side_result.at[arg],
+            result_send.at[arg],
+            result_recv.at[arg],
+            ep=side,
+        )
+
+    def outward_copy(arg, target, target_sem, to):
+        return remote(outward.at[arg], target, outward_send.at[arg], target_sem, ep=to)
+
+    own_heads = pl.ds(core * mine, mine)
+    state_copies = dict(
+        state=lambda: remote(
+            own_state, side_state, state_send.at[0], state_recv.at[0], ep=side
+        ),
+        decay=lambda: remote(
+            own_decay, side_decay, state_send.at[1], state_recv.at[1], ep=side
+        ),
+        before=lambda: remote(
+            before.at[own_heads],
+            before.at[own_heads],
+            state_send.at[2],
+            state_recv.at[2],
+            ep=side,
+        ),
+        chain=lambda: remote(
+            next_state, before.at[own_heads], state_send.at[3], state_recv.at[3], ep=me + 2
+        ),
+        mixed=lambda: remote(
+            mixed.at[partner], mixed_peer, mixed_send.at[0], mixed_recv.at[0], tp=partner
+        ),
+    )
+
+    copies[0].wait()
+    x = x_v[...].astype(f32)
+    normed = (
+        x * lax.rsqrt(jnp.mean(x * x, axis=1, keepdims=True) + EPSILON) * gain_ref[...]
+    ).astype(bf16)
+    for part in range(SPLIT):
+        rows[(chip * SPLIT + part) * 2 + core] = normed[part * part_rows : (part + 1) * part_rows]
+    score = score_ref[...]
+    weight = ROUTED_SCALE * score / jnp.sum(score, axis=1, keepdims=True)
+    lane = lax.broadcasted_iota(jnp.int32, (length, LANES), 1)
+    table = jnp.zeros((length, LANES), f32)
+    for k in range(score.shape[1]):
+        table = table + jnp.where(lane == index_ref[:, k : k + 1], weight[:, k : k + 1], 0.0)
+    gates[chip * 2 + core] = table.T[:count]
+
+    pl.semaphore_wait(barrier, 2 + has_right.astype(jnp.int32) + has_left.astype(jnp.int32))
 
     @pl.when(has_right)
     def _():
-        row_copy(x_ref, me, right_sem, me + 2).start()
+        table_copy(chip, table_right, me + 2).start()
 
     @pl.when(has_left)
     def _():
-        row_copy(x_ref, me, left_sem, me - 2).start()
-
-    row_copy(x_ref, me, side_sem, side).start()
-
-    copies[0].wait()
-    copies[1].wait()
-    gate_part = jnp.dot(
-        x_ref[:, :width], shared_gate_w[...], preferred_element_type=jnp.float32
-    )
-    up_part = jnp.dot(x_ref[:, :width], shared_up_w[...], preferred_element_type=jnp.float32)
-    own_hidden[count] = (jax.nn.silu(gate_part) * up_part).astype(jnp.bfloat16)
-    for copy in copies[2:]:
-        copy.wait()
-
-    def down(step, weight):
-        hidden_copy(step).wait_recv()
-        return jnp.dot(
-            own_hidden[step], weight[0], preferred_element_type=jnp.float32
-        ) + jnp.dot(peer_hidden[step], weight[1], preferred_element_type=jnp.float32)
-
-    def routed_down(step):
-        _, block = block_of(step)
-        place = pl.ds(pl.multiple_of(block * block_rows, block_rows), block_rows)
-        routed_ref[place, :] = down(step, down_w).astype(jnp.bfloat16)
-
-    def turn(step, _):
-        source, block = block_of(step)
-        odd = step % 2
-
-        @pl.when(step > 0)
-        def _():
-            row_copy(x_ref, block, side_sem, side).wait_recv()
-
-        @pl.when(jnp.logical_and(step > 0, odd == 0))
-        def _():
-            @pl.when(goes_right(source))
+        table_copy(chip, table_left, me - 2).start()
+
+    for part in range(SPLIT):
+        row_copy(chip * SPLIT + part, side_sem, side).start()
+    table_copy(chip, table_side, side).start()
+
+    def send_right(arg):
+        row_copy(arg, right_sem, me + 2).start()
+
+    def send_left(arg):
+        row_copy(arg, left_sem, me - 2).start()
+
+    def forward(arg):
+        source, part = arg // SPLIT, arg % SPLIT
+        arrived_row(arg * 2 + core)
+        to_right = jnp.logical_and(source < chip, has_right)
+        to_left = jnp.logical_and(source > chip, has_left)
+
+        @pl.when(part == 0)
+        def _():
+            arrived_table(source * 2 + core)
+
+            @pl.when(to_right)
             def _():
-                row_copy(rows.at[block], block, right_sem, me + 2).start()
-
-            @pl.when(goes_left(source))
+                table_copy(source, table_right, me + 2).start()
+
+            @pl.when(to_left)
             def _():
-                row_copy(rows.at[block], block, left_sem, me - 2).start()
-
-            row_copy(rows.at[block], block, side_sem, side).start()
-
-        x = rows[block, :, :width]
-        tail = rows[block, :, width:].astype(jnp.float32)
-        lane = lax.broadcasted_iota(jnp.int32, tail.shape, 1)
-        own_gate = jnp.sum(
-            jnp.where(lane % (LANES // 2) == me, tail, 0.0), axis=1, keepdims=True
+                table_copy(source, table_left, me - 2).start()
+
+            table_copy(source, table_side, side).start()
+
+        @pl.when(to_right)
+        def _():
+            send_right(arg)
+
+        @pl.when(to_left)
+        def _():
+            send_left(arg)
+
+        row_copy(arg, side_sem, side).start()
+
+    def mix_local(arg):
+        for i in (1, 2, 3):
+            copies[i].wait()
+        row = lax.broadcasted_iota(jnp.int32, (length, length), 0)
+        column = lax.broadcasted_iota(jnp.int32, (length, length), 1)
+        upper = row < BLK
+        left = column < BLK
+        causal = jnp.logical_and(row >= column, upper == left)
+        crossed = jnp.logical_and(jnp.logical_not(upper), left)
+        ones = causal.astype(f32).astype(bf16)
+        head_lane = lax.broadcasted_iota(jnp.int32, (length, heads), 1)
+        middle = BLK // 2 - 1
+
+        def one_head(h, _):
+            lanes = pl.ds(pl.multiple_of(h * HEAD_CHANNELS, HEAD_CHANNELS), HEAD_CHANNELS)
+            query = jax.nn.silu(query_v[:, lanes].astype(f32))
+            key = margin_ref[:, lanes] * jax.nn.sigmoid(-forget_v[:, lanes].astype(f32))
+            extra = jnp.sum(
+                jnp.where(head_lane == h, extra_ref[...], 0.0), axis=1, keepdims=True
+            )
+            decay = jnp.log1p(-key) + extra
+            high = decay.astype(bf16)
+            rest = decay - high.astype(f32)
+            mid = rest.astype(bf16)
+            low = (rest - mid.astype(f32)).astype(bf16)
+            total = dot(ones, high) + dot(ones, mid) + dot(ones, low)
+            center = jnp.where(upper, total[middle : middle + 1], total[BLK + middle : BLK + middle + 1])
+            end = jnp.where(upper, total[BLK - 1 : BLK], total[2 * BLK - 1 : 2 * BLK])
+            first = jnp.exp(total[BLK - 1 : BLK])
+            second = jnp.exp(total[2 * BLK - 1 : 2 * BLK])
+            query_end = query * jnp.exp(total)
+            key_end = key * jnp.exp(end - total)
+            near = dot_nt(
+                (query * jnp.exp(total - center)).astype(bf16),
+                (key * jnp.exp(center - total)).astype(bf16),
+            )
+            far = dot_nt(query_end.astype(bf16), key_end.astype(bf16))
+            scores = jnp.where(causal, near, jnp.where(crossed, far, 0.0)).astype(bf16)
+            value = value_v[:, lanes]
+            local_out[:, lanes] = dot(scores, value)
+            carried_query[:, lanes] = jnp.where(upper, query_end, query_end * first).astype(bf16)
+            key_state = jnp.where(upper, key_end * second, key_end).astype(bf16)
+            own_state[h] = dot_tn(value, key_state).astype(bf16)
+            own_decay[pl.ds(h, 1), :] = first * second
+            return 0
+
+        lax.fori_loop(0, heads, one_head, 0)
+        state_copies["state"]().start()
+        state_copies["decay"]().start()
+
+    def mix_state(arg):
+        state_copies["state"]().wait_recv()
+        state_copies["decay"]().wait_recv()
+
+        @pl.when(has_left)
+        def _():
+            state_copies["chain"]().wait_recv()
+            state_copies["before"]().start()
+
+        @pl.when(jnp.logical_not(has_left))
+        def _():
+            before[...] = jnp.zeros(before.shape, bf16)
+
+        @pl.when(has_right)
+        def _():
+            def one_head(i, _):
+                h = core * mine + i
+                own, beside = own_state[h].astype(f32), side_state[h].astype(f32)
+                own_d, beside_d = own_decay[pl.ds(h, 1), :], side_decay[pl.ds(h, 1), :]
+                state0 = jnp.where(core == 0, own, beside)
+                state1 = jnp.where(core == 0, beside, own)
+                decay1 = jnp.where(core == 0, beside_d, own_d)
+                carried = before[h].astype(f32) * (own_d * beside_d)
+                next_state[i] = (carried + decay1 * state0 + state1).astype(bf16)
+                return 0
+
+            lax.fori_loop(0, mine, one_head, 0)
+            state_copies["chain"]().start()
+
+    def mix_finish(arg):
+        copies[12].wait()
+        copies[13].wait()
+
+        @pl.when(has_left)
+        def _():
+            state_copies["before"]().wait_recv()
+
+        def one_head(h, _):
+            lanes = pl.ds(pl.multiple_of(h * HEAD_CHANNELS, HEAD_CHANNELS), HEAD_CHANNELS)
+            state = before[h].astype(f32)
+            beside = side_state[h].astype(f32)
+            later = side_decay[pl.ds(h, 1), :] * state + beside
+            state = jnp.where(core == 0, state, later).astype(bf16)
+            out = local_out[:, lanes] + dot_nt(carried_query[:, lanes], state)
+            factor = lax.rsqrt(jnp.mean(out * out, axis=1, keepdims=True) + EPSILON)
+            gate = jax.nn.silu(output_gate_v[:, lanes].astype(f32))
+            gated[:, lanes] = (out * factor * head_gain_ref[:, lanes] * gate).astype(bf16)
+            return 0
+
+        lax.fori_loop(0, heads, one_head, 0)
+        tile = 512
+        kept = length // 2
+
+        def one_tile(n, _):
+            lanes = pl.ds(pl.multiple_of(n * tile, tile), tile)
+            partial = dot(gated[...], out_weight_v[:, lanes]).astype(bf16)
+            mixed[0, :, lanes] = partial[:kept]
+            mixed[1, :, lanes] = partial[kept:]
+            return 0
+
+        lax.fori_loop(0, out_weight_v.shape[1] // tile, one_tile, 0)
+        state_copies["mixed"]().start()
+
+    def mix_out(arg):
+        state_copies["mixed"]().wait_recv()
+        recurrent_ref[...] = (mixed[half].astype(f32) + mixed_peer[...].astype(f32)).astype(bf16)
+
+    def hidden_part(arg):
+        shared = arg == routed
+        source, part = arg // SPLIT, arg % SPLIT
+
+        @pl.when(shared)
+        def _():
+            for i in range(4, 12):
+                copies[i].wait()
+
+        @pl.when(jnp.logical_not(shared))
+        def _():
+            arrived_row(arg * 2 + other)
+
+            @pl.when(part == 0)
+            def _():
+                arrived_table(source * 2 + other)
+
+        which = shared.astype(jnp.int32)
+        low = jnp.where(shared, chip * SPLIT * 2 + core, arg * 2)
+        high = jnp.where(shared, chip * SPLIT * 2 + core + 2, arg * 2 + 1)
+        x = jnp.concatenate([rows[low], rows[high]], axis=0)
+        lane = lax.broadcasted_iota(jnp.int32, (length, count), 1)
+        block_low = jnp.where(shared, chip * 2 + core, source * 2)
+        block_high = jnp.where(shared, chip * 2 + core, source * 2 + 1)
+
+        def own_gate(place):
+            column = jnp.sum(
+                jnp.where(lane == me, gates[place].T, 0.0), axis=1, keepdims=True
+            )
+            return jnp.where(part == 0, column[:part_rows], column[part_rows:])
+
+        routed_gate = jnp.concatenate([own_gate(block_low), own_gate(block_high)], axis=0)
+        scale = jnp.where(shared, 1.0, routed_gate)
+        gate_part = dot(x, gate_w[which])
+        up_part = dot(x, up_w[which])
+        own_hidden[arg] = (jax.nn.silu(gate_part) * up_part * scale).astype(bf16)
+        hidden_copy(arg).start()
+
+    def down_part(arg):
+        shared = arg == routed
+        which = shared.astype(jnp.int32)
+        hidden_copy(arg).wait_recv()
+        out = dot(own_hidden[arg], down_w[which, 0]) + dot(peer_hidden[arg], down_w[which, 1])
+        out = out.astype(bf16)
+        result[arg, 0] = out[:part_rows]
+        result[arg, 1] = out[part_rows:]
+
+        @pl.when(jnp.logical_not(shared))
+        def _():
+            result_copy(arg).start()
+
+    def chip_sum(arg):
+        result_copy(arg).wait_recv()
+        return result[arg, core].astype(f32) + side_result[arg].astype(f32)
+
+    def to_neighbour(arg):
+        source = arg // SPLIT
+        return source > chip, jnp.abs(source - chip) == 1
+
+    def outward_to(arg, place):
+        part = arg % SPLIT
+        target, sem, to = (
+            (inward_left.at[part], left_recv.at[part], me + 2),
+            (inward.at[arg], inward_recv.at[arg], me + 2),
+            (inward_right.at[part], right_recv.at[part], me - 2),
+            (inward.at[arg], inward_recv.at[arg], me - 2),
+        )[place]
+        return outward_copy(arg, target, sem, to)
+
+    def send_sum(arg):
+        right, adjacent = to_neighbour(arg)
+        inner = jnp.logical_and(has_left, has_right)
+        total = chip_sum(arg)
+
+        @pl.when(inner)
+        def _():
+            outward_to(arg, 1).wait_recv()
+            outward[arg] = (total + inward[arg].astype(f32)).astype(bf16)
+
+        @pl.when(jnp.logical_not(inner))
+        def _():
+            outward[arg] = total.astype(bf16)
+
+        far = jnp.logical_not(adjacent)
+        for place, (direction, distance) in enumerate(
+            (
+                (right, adjacent),
+                (right, far),
+                (jnp.logical_not(right), adjacent),
+                (jnp.logical_not(right), far),
+            )
+        ):
+
+            @pl.when(jnp.logical_and(direction, distance))
+            def _():
+                outward_to(arg, place).start()
+
+    def finish(arg):
+        part = arg % SPLIT
+        total = chip_sum(arg) + result[routed, part].astype(f32)
+        place = pl.ds(pl.multiple_of(part * part_rows, part_rows), part_rows)
+
+        @pl.when(has_left)
+        def _():
+            outward_to(arg, 0).wait_recv()
+
+        @pl.when(has_right)
+        def _():
+            outward_to(arg, 2).wait_recv()
+
+        from_left = jnp.where(has_left, inward_left[part].astype(f32), 0.0)
+        from_right = jnp.where(has_right, inward_right[part].astype(f32), 0.0)
+        expert_ref[place, :] = (total + from_left + from_right).astype(bf16)
+
+    actions = dict(
+        SR=send_right,
+        SL=send_left,
+        RF=forward,
+        MA=mix_local,
+        ST=mix_state,
+        H=hidden_part,
+        D=down_part,
+        S=send_sum,
+        FIN=finish,
+        MB=mix_finish,
+        MO=mix_out,
+    )
+    mine_words = []
+    for n in range(steps // 3):
+        word = jnp.int32(words[0][n])
+        for c in range(1, chips):
+            word = jnp.where(chip == c, words[c][n], word)
+        mine_words.append(word)
+
+    def turn(i, _):
+        place, digit = i // 3, i % 3
+        word = mine_words[0]
+        for n in range(1, steps // 3):
+            word = jnp.where(place == n, mine_words[n], word)
+        code = jnp.where(
+            digit == 0, word % 256, jnp.where(digit == 1, word // 256 % 256, word // 65536)
         )
-        gate_part = jnp.dot(x, gate_w[...], preferred_element_type=jnp.float32)
-        up_part = jnp.dot(x, up_w[...], preferred_element_type=jnp.float32)
-        own_hidden[step] = (jax.nn.silu(gate_part) * up_part * own_gate).astype(jnp.bfloat16)
-
-        @pl.when(step == 0)
-        def _():
-            hidden_copy(count).start()
-
-        @pl.when(step > 0)
-        def _():
-            routed_down(step - 1)
-
-        hidden_copy(step).start()
+        kind, arg = code // 16, code % 16
+        for name, action in actions.items():
+
+            @pl.when(kind == NUMBER[name])
+            def _():
+                action(arg)
+
         return 0
 
-    lax.fori_loop(0, count, turn, 0)
-    shared_ref[...] = down(count, shared_down_w)
-    routed_down(count - 1)
-
-    def finish(step, _):
-        source, block = block_of(step)
-        hidden_copy(step).wait_send()
-
-        @pl.when(step % 2 == 0)
-        def _():
-            @pl.when(goes_right(source))
+    lax.fori_loop(0, steps, turn, 0)
+
+    def drain(arg, _):
+        source, part = arg // SPLIT, arg % SPLIT
+        hidden_copy(arg).wait_send()
+        result_copy(arg).wait_send()
+        row_copy(arg, side_sem, side).wait_send()
+        to_right = jnp.logical_and(source <= chip, has_right)
+        to_left = jnp.logical_and(source >= chip, has_left)
+
+        @pl.when(to_right)
+        def _():
+            row_copy(arg, right_sem, me + 2).wait_send()
+
+        @pl.when(to_left)
+        def _():
+            row_copy(arg, left_sem, me - 2).wait_send()
+
+        @pl.when(source != chip)
+        def _():
+            outward_copy(arg, inward.at[arg], inward_recv.at[arg], side).wait_send()
+
+        @pl.when(part == 0)
+        def _():
+            table_copy(source, table_side, side).wait_send()
+
+            @pl.when(to_right)
             def _():
-                row_copy(x_ref, block, right_sem, me + 2).wait_send()
-
-            @pl.when(goes_left(source))
+                table_copy(source, table_right, me + 2).wait_send()
+
+            @pl.when(to_left)
             def _():
-                row_copy(x_ref, block, left_sem, me - 2).wait_send()
-
-            row_copy(x_ref, block, side_sem, side).wait_send()
+                table_copy(source, table_left, me - 2).wait_send()
 
         return 0
 
-    lax.fori_loop(0, count, finish, 0)
-    hidden_copy(count).wait_send()
-
-
-def dense_expert_half(
+    lax.fori_loop(0, routed, drain, 0)
+    hidden_copy(routed).wait_send()
+    state_copies["state"]().wait_send()
+    state_copies["decay"]().wait_send()
+
+    @pl.when(has_left)
+    def _():
+        state_copies["before"]().wait_send()
+
+    @pl.when(has_right)
+    def _():
+        state_copies["chain"]().wait_send()
+
+    state_copies["mixed"]().wait_send()
+
+
+def fused_fits(position_decay_extra, chosen_expert_index, routed_gate_weight):
+    count, tensor = lax.axis_size("ep"), lax.axis_size("tp")
+    length, heads = position_decay_extra.shape
+    tokens, top = chosen_expert_index.shape
+    every_row_fits = 2 * top >= count and routed_gate_weight.shape[0] == 1
+    sizes = length == tokens == 2 * BLK and heads % 2 == 0
+    return every_row_fits and sizes and tensor == 2 and count % 2 == 0 and count == 2 * len(ORDERS)
+
+
+def fused_layer(
+    recurrence_query_input,
+    forget_gate_input,
+    recurrence_value_input,
+    output_gate_input,
+    forget_lower_margin,
+    position_decay_extra,
+    head_norm_gain,
+    recurrence_out_weight,
     expert_hidden_state,
     chosen_expert_index,
     chosen_expert_score,
@@ -408,73 +878,112 @@
     shared_up_weight,
     shared_down_weight,
 ):
-    tokens = chosen_expert_index.shape[0]
+    f32, bf16 = jnp.float32, jnp.bfloat16
     count = lax.axis_size("ep")
-    features = expert_hidden_state.astype(jnp.float32)
-    width = features.shape[1]
-    units, width_out = routed_gate_weight.shape[2], routed_down_weight.shape[2]
-    normed = (
-        features
-        * lax.rsqrt(jnp.mean(features * features, axis=1, keepdims=True) + EPSILON)
-        * expert_norm_gain[None, :]
-    ).astype(jnp.bfloat16)
-    gates = ROUTED_SCALE * chosen_expert_score / jnp.sum(chosen_expert_score, axis=1, keepdims=True)
-    slots = LANES // 2
-    chosen = chosen_expert_index[:, :, None] == jnp.arange(slots, dtype=jnp.int32)[None, None, :]
-    gate_table = jnp.sum(jnp.where(chosen, gates[:, :, None], 0.0), axis=1)
-    high = gate_table.astype(jnp.bfloat16)
-    low = (gate_table - high.astype(jnp.float32)).astype(jnp.bfloat16)
-    sent = jnp.concatenate([normed, high, low], axis=1)
+    chips = count // 2
+    routed = chips * SPLIT
+    length, channels = recurrence_query_input.shape
+    heads = position_decay_extra.shape[1]
+    width, width_out = expert_hidden_state.shape[1], recurrence_out_weight.shape[1]
+    units, features = routed_gate_weight.shape[2], routed_down_weight.shape[2]
+    part_rows = length // SPLIT
     hbm = pl.BlockSpec(memory_space=pl.ANY)
     vmem = pl.BlockSpec(memory_space=pltpu.VMEM)
-    weight = pltpu.VMEM((width, units), jnp.bfloat16)
-    down_weight = pltpu.VMEM((2, units, width_out), jnp.bfloat16)
-    hidden = pltpu.VMEM((count + 1, tokens, units), jnp.bfloat16)
-    block_sems = pltpu.SemaphoreType.DMA((count,))
-    routed, shared = pl.pallas_call(
-        functools.partial(expert_kernel, count),
+    dma = pltpu.SemaphoreType.DMA
+    mixer_rows = pltpu.VMEM((length, channels), bf16)
+    hidden = pltpu.VMEM((routed + 1, 2 * part_rows, units), bf16)
+    partial = pltpu.VMEM((routed, part_rows, features), bf16)
+    edge = pltpu.VMEM((SPLIT, part_rows, features), bf16)
+    state = pltpu.VMEM((heads, HEAD_CHANNELS, HEAD_CHANNELS), bf16)
+    decay = pltpu.VMEM((heads, HEAD_CHANNELS), f32)
+    return pl.pallas_call(
+        functools.partial(fused_kernel, count),
         out_shape=(
-            jax.ShapeDtypeStruct((count * tokens, width_out), jnp.bfloat16),
-            jax.ShapeDtypeStruct((tokens, width_out), jnp.float32),
+            jax.ShapeDtypeStruct((length // 2, width_out), bf16),
+            jax.ShapeDtypeStruct((length, features), bf16),
         ),
-        in_specs=[vmem] + [hbm] * 6,
+        in_specs=[hbm] * 12 + [vmem] * 6,
         out_specs=(vmem, vmem),
         scratch_shapes=[
-            pltpu.VMEM((count, tokens, width + LANES), jnp.bfloat16),
-            weight,
-            weight,
-            down_weight,
-            weight,
-            weight,
-            down_weight,
+            mixer_rows,
+            mixer_rows,
+            mixer_rows,
+            mixer_rows,
+            pltpu.VMEM(recurrence_out_weight.shape, bf16),
+            pltpu.VMEM((length, width), bf16),
+            pltpu.VMEM((2, width, units), bf16),
+            pltpu.VMEM((2, width, units), bf16),
+            pltpu.VMEM((2, 2, units, features), bf16),
+            pltpu.VMEM((routed * 2, part_rows, width), bf16),
+            pltpu.VMEM((count, count, length), f32),
             hidden,
             hidden,
-            pltpu.SemaphoreType.DMA((9,)),
-            block_sems,
-            block_sems,
-            block_sems,
-            block_sems,
-            pltpu.SemaphoreType.DMA((count + 1,)),
-            pltpu.SemaphoreType.DMA((count + 1,)),
+            pltpu.VMEM((routed + 1, 2, part_rows, features), bf16),
+            partial,
+            partial,
+            edge,
+            edge,
+            partial,
+            pltpu.VMEM((length, channels), f32),
+            mixer_rows,
+            state,
+            decay,
+            state,
+            decay,
+            state,
+            pltpu.VMEM((heads // 2, HEAD_CHANNELS, HEAD_CHANNELS), bf16),
+            mixer_rows,
+            pltpu.VMEM((2, length // 2, width_out), bf16),
+            pltpu.VMEM((length // 2, width_out), bf16),
+            dma((14,)),
+            dma((routed * 2,)),
+            dma((count,)),
+            dma((routed,)),
+            dma((routed,)),
+            dma((routed,)),
+            dma((chips,)),
+            dma((chips,)),
+            dma((chips,)),
+            dma((routed + 1,)),
+            dma((routed + 1,)),
+            dma((routed,)),
+            dma((routed,)),
+            dma((routed,)),
+            dma((routed,)),
+            dma((SPLIT,)),
+            dma((SPLIT,)),
+            dma((4,)),
+            dma((4,)),
+            dma((1,)),
+            dma((1,)),
         ],
         compiler_params=pltpu.CompilerParams(
-            collective_id=0, has_side_effects=True, vmem_limit_bytes=48 * 1024 * 1024
+            collective_id=0, has_side_effects=True, vmem_limit_bytes=56 * 1024 * 1024
         ),
         cost_estimate=pl.CostEstimate(
-            flops=45_000_000_000, bytes_accessed=16_000_000, transcendentals=0
+            flops=9_000_000_000, bytes_accessed=18_000_000, transcendentals=0
         ),
-        name="expert_kernel",
+        name="fused_kernel",
     )(
-        sent,
+        recurrence_query_input,
+        forget_gate_input,
+        recurrence_value_input,
+        output_gate_input,
+        recurrence_out_weight,
+        expert_hidden_state,
         routed_gate_weight,
         routed_up_weight,
         routed_down_weight,
         shared_gate_weight,
         shared_up_weight,
         shared_down_weight,
-    )
-    total = lax.psum_scatter(routed, "ep", scatter_dimension=0, tiled=True)
-    return (shared + total.astype(jnp.float32)).astype(jnp.bfloat16)
+        forget_lower_margin[None, :],
+        position_decay_extra,
+        head_norm_gain[None, :],
+        chosen_expert_index,
+        chosen_expert_score,
+        expert_norm_gain[None, :],
+    )
 
 
 def per_device(
@@ -497,6 +1006,27 @@
     shared_up_weight,
     shared_down_weight,
 ):
+    if fused_fits(position_decay_extra, chosen_expert_index, routed_gate_weight):
+        return fused_layer(
+            recurrence_query_input,
+            forget_gate_input,
+            recurrence_value_input,
+            output_gate_input,
+            forget_lower_margin,
+            position_decay_extra,
+            head_norm_gain,
+            recurrence_out_weight,
+            expert_hidden_state,
+            chosen_expert_index,
+            chosen_expert_score,
+            expert_norm_gain,
+            routed_gate_weight,
+            routed_up_weight,
+            routed_down_weight,
+            shared_gate_weight,
+            shared_up_weight,
+            shared_down_weight,
+        )
     recurrence_output = mixer_half(
         recurrence_query_input,
         forget_gate_input,
@@ -507,11 +1037,7 @@
         head_norm_gain,
         recurrence_out_weight,
     )
-    tokens, top = chosen_expert_index.shape
-    experts = routed_gate_weight.shape[0] * lax.axis_size("ep")
-    every_row_fits = 2 * top >= experts and routed_gate_weight.shape[0] == 1 and experts <= 64
-    half = dense_expert_half if every_row_fits else expert_half
-    expert_out = half(
+    expert_out = expert_half(
         expert_hidden_state,
         chosen_expert_index,
         chosen_expert_score,

time: 136 us -> 76.5 us (0.56)
  waiting for transfers between devices: 24 us -> 0 us
  between operations: 14.5 us -> 0.64 us
  other arithmetic: 11 us -> 0 us
  Pallas kernels: 75.2 us -> 68 us
  matrix products: 4.39 us -> 0 us
  local copies, waits for them, and re-layouts: 4.37 us -> 7.59 us
  starting transfers between devices: 2.41 us -> 0 us
    reduce_scatter x1 -> x0, waiting for transfers between devices: 23.9 us -> none  [dense_expert_half(): total = lax.psum_scatter(routed, 'ep', scatter_dimension=0, tiled=True)]
    pallas_call x1, Pallas kernels: 75.2 us -> 68 us  [fused_layer(): pl.pallas_call(functools.partial(fused_kernel, count), out_shape=(jax.Sha...]
    unnamed x33 -> x5, local copies, waits for them, and re-layouts: 2.35 us -> 7.59 us
    convert_element_type x6 -> x0, other arithmetic: 5.12 us -> none  [the longest x1 1.84 us: carried_in(): part = everything[k].astype(jnp.float32)]
    dot_general x4 -> x0, matrix products: 4.39 us -> none  [the longest x1 3.08 us: mixer_half(): jnp.dot(gated_rows, recurrence_out_weight, preferred_element_type=jnp.flo...]
    ppermute x1 -> x0, starting transfers between devices: 2.33 us -> none  [mixer_half(): received = lax.ppermute(sent, 'tp', [(0, 1), (1, 0)])]
    another operation x4 -> x0, other arithmetic: 1.88 us -> none
    unnamed x2 -> x0, other arithmetic: 1.46 us -> none
  transfers between devices with their start and end apart: 3 -> 0, of which waited for: 1 -> 0; matrix products, arithmetic and copies ran while one was open for 9% -> 0% of each run, Pallas kernels for 55% -> 0%
where the time goes in v1:
time: 76.5 us; the launch traced here: 76.2 us
  Pallas kernels  68 us (89%)
  local copies, waits for them, and re-layouts  7.59 us (10%)
    pallas_call x1, Pallas kernels, fused_layer(): pl.pallas_call(functools.partial(fused_kernel, count), out_shape=(jax.Sha...  68 us
    unnamed x5, local copies, waits for them, and re-layouts  7.59 us

profile of v1, /device:TPU:0, one launch (start us, length us, event | category | flops | bytes accessed | tf_op | source)
XLA Modules:
  0.0 76.2 jit_solution(11132416798782897433)
XLA Ops:
  0.6 1.4 %copy.20.extra_ref = f32[128,8]{1,0:T(8,128)} copy(f32[128,8]{0,1:T(8,128)} %param.23) | data formatting | bytes 8192 | tf_op args[5]
  2.0 1.4 %copy.21.index_ref = s32[128,4]{1,0:T(8,128)} copy(s32[128,4]{0,1:T(4,128)} %param.27) | data formatting | bytes 4096 | tf_op args[9]
  3.5 1.4 %copy.22.score_ref = f32[128,4]{1,0:T(8,128)} copy(f32[128,4]{0,1:T(4,128)} %param.28) | data formatting | bytes 4096 | tf_op args[10]
  4.9 68.0 %fused_kernel.1 = (bf16[64,2048]{1,0:T(8,128)(2,1)}, bf16[128,1024]{1,0:T(8,128)(2,1)}) custom-call(bf16[128,1024]{1,0:T(8,128)(2,1)} %query_hbm.1, bf16[128,1024]{1,0:T(8,128)(2,1)} %forget_hbm.1, bf16[128,1024]{1,0:T(8,128)(2,1)} %value_hbm.1, bf16[128,1024]{1,0:T(8,128)(2,1)} %output_gate_hbm.1, bf16[1024,2048]{1,0:T(8,128)(2,1)} %out_weight_hbm.1, ...), custom_call_target="tpu_custom_call" | custom-call | flops 8999999488 | bytes 18000000 | tf_op jit(solution)/shard_map/fused_kernel/pallas_call | solution.py:899
  72.9 1.7 %copy.25 = bf16[64,2048]{1,0:T(8,128)(2,1)} copy(bf16[64,2048]{1,0:T(8,128)(2,1)} %get-tuple-element.4) | data formatting | bytes 524288
  74.5 1.7 %copy.26 = bf16[128,1024]{1,0:T(8,128)(2,1)} copy(bf16[128,1024]{1,0:T(8,128)(2,1)} %get-tuple-element.5) | data formatting | bytes 524288

commit v2 on v1

--- a/solution.py
+++ b/solution.py
@@ -188,47 +188,95 @@
 
 MESH = pl.DeviceIdType.MESH
 LANES = 128
-SPLIT = 2
-KINDS = ("NO", "SR", "SL", "RF", "MA", "ST", "H", "D", "S", "FIN", "MB", "MO")
+SPLIT = 4
+COARSE = 2
+GROUP = SPLIT // COARSE
+CROSSED = True
+KINDS = (
+    "NO",
+    "SR",
+    "SL",
+    "RF",
+    "RX",
+    "MA",
+    "ST",
+    "H",
+    "D",
+    "S",
+    "SX",
+    "FIN",
+    "FL",
+    "FR",
+    "FB",
+    "MB",
+    "MP",
+    "MO",
+)
 NUMBER = {name: place for place, name in enumerate(KINDS)}
 
 
 ORDERS = (
     (
-        ("SR", 0, 0), ("SR", 0, 1), ("MA", 0, 0), ("H", 4, 0), ("H", 0, 0), ("ST", 0, 0),
-        ("H", 0, 1), ("MB", 0, 0), ("RF", 1, 0), ("D", 4, 0), ("D", 0, 0), ("H", 1, 0),
-        ("RF", 1, 1), ("D", 0, 1), ("H", 1, 1), ("RF", 2, 0), ("MO", 0, 0), ("H", 2, 0),
-        ("D", 1, 0), ("RF", 2, 1), ("S", 1, 0), ("D", 1, 1), ("H", 2, 1), ("S", 1, 1),
-        ("D", 2, 0), ("RF", 3, 0), ("S", 2, 0), ("H", 3, 0), ("D", 2, 1), ("S", 2, 1),
-        ("RF", 3, 1), ("H", 3, 1), ("D", 3, 0), ("S", 3, 0), ("D", 3, 1), ("S", 3, 1),
-        ("FIN", 0, 0), ("FIN", 0, 1),
+        ("SR", 0, 1, 0), ("SR", 0, 0, 0), ("SR", 0, 2, 0), ("H", 4, 0, 0), ("MA", 0, 0, 0),
+        ("MA", 0, 1, 0), ("MA", 0, 2, 0), ("MA", 0, 3, 0), ("H", 0, 0, 0), ("H", 0, 2, 0),
+        ("ST", 0, 0, 0), ("SR", 0, 3, 0), ("D", 4, 0, 0), ("MB", 0, 0, 0), ("MB", 0, 1, 0),
+        ("MB", 0, 2, 0), ("RX", 1, 0, 1), ("D", 0, 0, 0), ("RF", 2, 0, 0), ("D", 0, 2, 0),
+        ("RX", 1, 1, 1), ("RF", 1, 2, 1), ("H", 1, 0, 1), ("RF", 2, 1, 0), ("H", 2, 0, 0),
+        ("RF", 1, 3, 1), ("RF", 3, 0, 0), ("H", 1, 2, 1), ("D", 1, 2, 1), ("RF", 3, 1, 0),
+        ("S", 1, 2, 1), ("S", 1, 3, 1), ("H", 3, 0, 0), ("D", 2, 0, 0), ("RF", 3, 2, 0),
+        ("S", 2, 0, 0), ("S", 2, 1, 0), ("RF", 3, 3, 0), ("H", 3, 2, 0), ("D", 3, 0, 0),
+        ("RF", 2, 2, 0), ("S", 3, 0, 0), ("SX", 3, 1, 0), ("RF", 2, 3, 0), ("MB", 0, 3, 0),
+        ("MP", 0, 0, 0), ("MP", 0, 1, 0), ("H", 2, 2, 0), ("D", 3, 2, 0), ("MP", 0, 2, 0),
+        ("MP", 0, 3, 0), ("S", 3, 2, 0), ("S", 3, 3, 0), ("D", 1, 0, 1), ("S", 1, 0, 1),
+        ("S", 1, 1, 1), ("D", 2, 2, 0), ("S", 2, 2, 0), ("S", 2, 3, 0), ("MO", 0, 0, 0),
+        ("FR", 0, 2, 0), ("FIN", 0, 0, 0), ("FR", 0, 3, 0), ("FIN", 0, 1, 0),
     ),
     (
-        ("SL", 1, 0), ("SR", 1, 0), ("SL", 1, 1), ("SR", 1, 1), ("MA", 0, 0), ("H", 4, 0),
-        ("H", 1, 0), ("H", 1, 1), ("RF", 0, 0), ("RF", 2, 0), ("D", 4, 0), ("H", 0, 0),
-        ("H", 2, 0), ("D", 1, 0), ("RF", 0, 1), ("RF", 2, 1), ("D", 1, 1), ("H", 0, 1),
-        ("ST", 0, 0), ("H", 2, 1), ("D", 0, 0), ("RF", 3, 0), ("MB", 0, 0), ("D", 2, 0),
-        ("H", 3, 0), ("D", 0, 1), ("RF", 3, 1), ("D", 2, 1), ("H", 3, 1), ("MO", 0, 0),
-        ("D", 3, 0), ("S", 2, 0), ("D", 3, 1), ("FIN", 1, 0), ("S", 2, 1), ("FIN", 1, 1),
-        ("S", 3, 0), ("S", 3, 1), ("S", 0, 0), ("S", 0, 1),
+        ("SR", 1, 0, 0), ("SR", 1, 1, 0), ("SR", 1, 2, 0), ("H", 4, 0, 0), ("MA", 0, 0, 0),
+        ("H", 1, 0, 0), ("H", 1, 2, 0), ("SL", 1, 0, 1), ("MA", 0, 1, 0), ("MA", 0, 2, 0),
+        ("MA", 0, 3, 0), ("RF", 2, 0, 0), ("D", 4, 0, 0), ("SL", 1, 1, 1), ("RF", 0, 0, 0),
+        ("RF", 0, 1, 0), ("RF", 2, 1, 0), ("D", 1, 0, 0), ("H", 0, 0, 0), ("H", 2, 0, 0),
+        ("RF", 3, 0, 0), ("D", 1, 2, 0), ("RF", 0, 2, 0), ("RF", 3, 1, 0), ("D", 0, 0, 0),
+        ("RF", 0, 3, 0), ("SR", 1, 3, 0), ("ST", 0, 0, 0), ("H", 3, 0, 0), ("H", 0, 2, 0),
+        ("D", 2, 0, 0), ("MB", 0, 0, 0), ("RF", 3, 2, 0), ("MB", 0, 1, 0), ("MB", 0, 2, 0),
+        ("RF", 3, 3, 0), ("MB", 0, 3, 0), ("MP", 0, 0, 0), ("MP", 0, 1, 0), ("H", 3, 2, 0),
+        ("D", 3, 0, 0), ("RF", 2, 2, 0), ("MP", 0, 2, 0), ("MP", 0, 3, 0), ("D", 0, 2, 0),
+        ("RF", 2, 3, 0), ("SX", 0, 2, 0), ("SX", 0, 3, 0), ("H", 2, 2, 0), ("D", 3, 2, 0),
+        ("S", 2, 0, 0), ("S", 2, 1, 0), ("MO", 0, 0, 0), ("S", 3, 0, 0), ("D", 2, 2, 0),
+        ("SX", 3, 1, 0), ("S", 3, 2, 0), ("S", 0, 0, 0), ("S", 3, 3, 0), ("S", 0, 1, 0),
+        ("S", 2, 2, 0), ("S", 2, 3, 0), ("FIN", 1, 2, 1), ("FIN", 1, 0, 1), ("FIN", 1, 1, 1),
+        ("FIN", 1, 3, 1),
     ),
     (
-        ("SR", 2, 0), ("SL", 2, 0), ("SR", 2, 1), ("SL", 2, 1), ("MA", 0, 0), ("H", 4, 0),
-        ("H", 2, 0), ("H", 2, 1), ("RF", 3, 0), ("RF", 1, 0), ("D", 4, 0), ("H", 3, 0),
-        ("H", 1, 0), ("D", 2, 0), ("RF", 3, 1), ("RF", 1, 1), ("D", 2, 1), ("H", 3, 1),
-        ("H", 1, 1), ("D", 3, 0), ("RF", 0, 0), ("D", 1, 0), ("H", 0, 0), ("D", 3, 1),
-        ("RF", 0, 1), ("D", 1, 1), ("H", 0, 1), ("ST", 0, 0), ("D", 0, 0), ("MB", 0, 0),
-        ("D", 0, 1), ("S", 1, 0), ("MO", 0, 0), ("S", 1, 1), ("FIN", 2, 0), ("FIN", 2, 1),
-        ("S", 0, 0), ("S", 3, 0), ("S", 0, 1), ("S", 3, 1),
+        ("H", 4, 0, 0), ("SL", 2, 0, 0), ("SL", 2, 1, 0), ("SR", 2, 1, 1), ("MA", 0, 0, 0),
+        ("H", 2, 0, 0), ("H", 2, 2, 0), ("MA", 0, 1, 0), ("MA", 0, 2, 0), ("RF", 1, 0, 0),
+        ("SR", 2, 0, 1), ("RF", 3, 0, 0), ("MA", 0, 3, 0), ("D", 4, 0, 0), ("RF", 1, 1, 0),
+        ("D", 2, 0, 0), ("H", 1, 0, 0), ("RF", 3, 1, 0), ("D", 2, 2, 0), ("H", 3, 0, 0),
+        ("RF", 0, 0, 0), ("RF", 3, 2, 0), ("RF", 3, 3, 0), ("SL", 2, 2, 0), ("SL", 2, 3, 0),
+        ("H", 3, 2, 0), ("D", 1, 0, 0), ("RF", 0, 1, 0), ("RF", 1, 2, 0), ("D", 3, 0, 0),
+        ("H", 0, 0, 0), ("RF", 0, 2, 0), ("D", 3, 2, 0), ("RF", 0, 3, 0), ("H", 0, 2, 0),
+        ("RF", 1, 3, 0), ("D", 0, 0, 0), ("H", 1, 2, 0), ("ST", 0, 0, 0), ("MB", 0, 0, 0),
+        ("MB", 0, 1, 0), ("MB", 0, 2, 0), ("MB", 0, 3, 0), ("D", 0, 2, 0), ("MP", 0, 0, 0),
+        ("MP", 0, 1, 0), ("MP", 0, 2, 0), ("MP", 0, 3, 0), ("SX", 0, 2, 0), ("SX", 0, 3, 0),
+        ("D", 1, 2, 0), ("S", 1, 0, 0), ("S", 1, 1, 0), ("S", 0, 0, 0), ("MO", 0, 0, 0),
+        ("S", 0, 1, 0), ("S", 3, 0, 0), ("SX", 3, 1, 0), ("S", 3, 2, 0), ("S", 3, 3, 0),
+        ("S", 1, 2, 0), ("S", 1, 3, 0), ("FIN", 2, 2, 1), ("FIN", 2, 3, 1), ("FIN", 2, 0, 1),
+        ("FIN", 2, 1, 1),
     ),
     (
-        ("SL", 3, 0), ("SL", 3, 1), ("MA", 0, 0), ("H", 4, 0), ("H", 3, 0), ("H", 3, 1),
-        ("RF", 2, 0), ("D", 4, 0), ("H", 2, 0), ("D", 3, 0), ("RF", 2, 1), ("D", 3, 1),
-        ("H", 2, 1), ("D", 2, 0), ("RF", 1, 0), ("S", 2, 0), ("H", 1, 0), ("D", 2, 1),
-        ("S", 2, 1), ("RF", 1, 1), ("H", 1, 1), ("D", 1, 0), ("S", 1, 0), ("RF", 0, 0),
-        ("H", 0, 0), ("D", 1, 1), ("S", 1, 1), ("RF", 0, 1), ("H", 0, 1), ("ST", 0, 0),
-        ("D", 0, 0), ("MB", 0, 0), ("S", 0, 0), ("D", 0, 1), ("S", 0, 1), ("MO", 0, 0),
-        ("FIN", 3, 0), ("FIN", 3, 1),
+        ("SL", 3, 0, 0), ("SL", 3, 3, 0), ("SL", 3, 1, 0), ("SL", 3, 2, 0), ("H", 4, 0, 0),
+        ("MA", 0, 0, 0), ("MA", 0, 1, 0), ("H", 3, 0, 0), ("H", 3, 2, 0), ("MA", 0, 2, 0),
+        ("MA", 0, 3, 0), ("D", 4, 0, 0), ("D", 3, 0, 0), ("RF", 1, 0, 0), ("D", 3, 2, 0),
+        ("RX", 2, 0, 1), ("RX", 2, 1, 1), ("RF", 1, 1, 0), ("H", 2, 0, 1), ("H", 1, 0, 0),
+        ("RF", 2, 2, 1), ("RF", 0, 0, 0), ("RF", 2, 3, 1), ("RF", 0, 1, 0), ("H", 2, 2, 1),
+        ("H", 0, 0, 0), ("D", 2, 2, 1), ("RF", 1, 2, 0), ("S", 2, 2, 1), ("S", 2, 3, 1),
+        ("D", 1, 0, 0), ("RF", 0, 2, 0), ("S", 1, 0, 0), ("S", 1, 1, 0), ("D", 2, 0, 1),
+        ("RF", 0, 3, 0), ("S", 2, 0, 1), ("S", 2, 1, 1), ("H", 0, 2, 0), ("D", 0, 0, 0),
+        ("RF", 1, 3, 0), ("S", 0, 0, 0), ("S", 0, 1, 0), ("H", 1, 2, 0), ("ST", 0, 0, 0),
+        ("MB", 0, 0, 0), ("D", 0, 2, 0), ("MB", 0, 1, 0), ("MB", 0, 2, 0), ("MB", 0, 3, 0),
+        ("MP", 0, 0, 0), ("SX", 0, 2, 0), ("SX", 0, 3, 0), ("MP", 0, 1, 0), ("MP", 0, 2, 0),
+        ("MP", 0, 3, 0), ("D", 1, 2, 0), ("S", 1, 2, 0), ("S", 1, 3, 0), ("FIN", 3, 0, 0),
+        ("FL", 3, 1, 0), ("MO", 0, 0, 0), ("FIN", 3, 2, 0), ("FIN", 3, 3, 0),
     ),
 )
 
@@ -240,13 +288,16 @@
 def packed_orders(chips):
     orders = chip_orders(chips)
     steps = max(len(order) for order in orders)
-    steps = -(-steps // 3) * 3
+    steps = -(-steps // 2) * 2
     words = []
     for order in orders:
-        codes = [NUMBER[kind] * 16 + source * SPLIT + part for kind, source, part in order]
+        codes = [
+            (NUMBER[kind] * 64 + source * SPLIT + part) * 2 + turned
+            for kind, source, part, turned in order
+        ]
         codes = codes + [0] * (steps - len(codes))
         words.append(
-            [codes[i] + 256 * codes[i + 1] + 65536 * codes[i + 2] for i in range(0, steps, 3)]
+            [codes[i] + 32768 * codes[i + 1] for i in range(0, steps, 2)]
         )
     return steps, words
 
@@ -277,14 +328,20 @@
     shared_gate_hbm,
     shared_up_hbm,
     shared_down_hbm,
+    margin_hbm,
+    extra_hbm,
+    head_gain_hbm,
+    index_hbm,
+    score_hbm,
+    gain_hbm,
+    recurrent_ref,
+    expert_ref,
     margin_ref,
     extra_ref,
     head_gain_ref,
     index_ref,
     score_ref,
     gain_ref,
-    recurrent_ref,
-    expert_ref,
     query_v,
     forget_v,
     value_v,
@@ -301,8 +358,7 @@
     result,
     side_result,
     inward,
-    inward_left,
-    inward_right,
+    final,
     outward,
     local_out,
     carried_query,
@@ -321,6 +377,7 @@
     right_sem,
     left_sem,
     side_sem,
+    cross_sem,
     table_right,
     table_left,
     table_side,
@@ -330,8 +387,7 @@
     result_recv,
     outward_send,
     inward_recv,
-    left_recv,
-    right_recv,
+    final_recv,
     state_send,
     state_recv,
     mixed_send,
@@ -347,50 +403,59 @@
     partner = 1 - half
     has_right, has_left = chip < chips - 1, chip > 0
     length = query_v.shape[0]
-    heads = extra_ref.shape[1]
+    heads = extra_ref.shape[0]
     mine = heads // 2
     part_rows = rows.shape[1]
     units = gate_w.shape[2]
     routed = chips * SPLIT
+    last = chips * COARSE
+    coarse_rows = GROUP * part_rows
+    tiles = 4
+    tile = out_weight_v.shape[1] // tiles
     steps, words = packed_orders(chips)
 
     def half_rows(ref, which):
         return ref.at[pl.ds(pl.multiple_of(which * units, units), units), :]
 
-    loads = [
-        (x_hbm, x_v),
-        (forget_hbm, forget_v),
-        (query_hbm, query_v),
-        (value_hbm, value_v),
-        (shared_gate_hbm, gate_w.at[1]),
-        (shared_up_hbm, up_w.at[1]),
-        (gate_hbm.at[0], gate_w.at[0]),
-        (up_hbm.at[0], up_w.at[0]),
-        (half_rows(shared_down_hbm, half), down_w.at[1, 0]),
-        (half_rows(shared_down_hbm, partner), down_w.at[1, 1]),
-        (half_rows(down_hbm.at[0], half), down_w.at[0, 0]),
-        (half_rows(down_hbm.at[0], partner), down_w.at[0, 1]),
-        (output_gate_hbm, output_gate_v),
-        (out_weight_hbm, out_weight_v),
-    ]
-    copies = [
-        pltpu.make_async_copy(source, target, load_sem.at[i])
-        for i, (source, target) in enumerate(loads)
-    ]
-    for copy in copies:
+    loads = dict(
+        x=(x_hbm, x_v),
+        gain=(gain_hbm, gain_ref),
+        index=(index_hbm, index_ref),
+        score=(score_hbm, score_ref),
+        shared_gate=(shared_gate_hbm, gate_w.at[1]),
+        shared_up=(shared_up_hbm, up_w.at[1]),
+        forget=(forget_hbm, forget_v),
+        query=(query_hbm, query_v),
+        value=(value_hbm, value_v),
+        margin=(margin_hbm, margin_ref),
+        extra=(extra_hbm, extra_ref),
+        gate=(gate_hbm.at[0], gate_w.at[0]),
+        up=(up_hbm.at[0], up_w.at[0]),
+        shared_down0=(half_rows(shared_down_hbm, half), down_w.at[1, 0]),
+        shared_down1=(half_rows(shared_down_hbm, partner), down_w.at[1, 1]),
+        down0=(half_rows(down_hbm.at[0], half), down_w.at[0, 0]),
+        down1=(half_rows(down_hbm.at[0], partner), down_w.at[0, 1]),
+        output_gate=(output_gate_hbm, output_gate_v),
+        head_gain=(head_gain_hbm, head_gain_ref),
+        out_weight=(out_weight_hbm, out_weight_v),
+    )
+    copies = {
+        name: pltpu.make_async_copy(source, target, load_sem.at[i])
+        for i, (name, (source, target)) in enumerate(loads.items())
+    }
+    for copy in copies.values():
         copy.start()
+
+    def loaded(*names):
+        for name in names:
+            copies[name].wait()
 
     barrier = pltpu.get_barrier_semaphore()
     pl.semaphore_signal(barrier, inc=1, device_id={"ep": side}, device_id_type=MESH)
     pl.semaphore_signal(barrier, inc=1, device_id={"tp": partner}, device_id_type=MESH)
-
-    @pl.when(has_right)
-    def _():
-        pl.semaphore_signal(barrier, inc=1, device_id={"ep": me + 2}, device_id_type=MESH)
-
-    @pl.when(has_left)
-    def _():
-        pl.semaphore_signal(barrier, inc=1, device_id={"ep": me - 2}, device_id_type=MESH)
+    for distance in range(1, chips):
+        there = (chip + distance) % chips * 2 + core
+        pl.semaphore_signal(barrier, inc=1, device_id={"ep": there}, device_id_type=MESH)
 
     def remote(source, target, send, recv, **device):
         return pltpu.make_async_remote_copy(
@@ -405,6 +470,12 @@
     def row_copy(arg, sems, target):
         block = arg * 2 + core
         return remote(rows.at[block], rows.at[block], sems.at[arg], row_sem.at[block], ep=target)
+
+    def cross_copy(arg):
+        block = arg * 2 + core
+        return remote(
+            rows.at[block], rows.at[block], cross_sem.at[arg], row_sem.at[block], tp=partner
+        )
 
     def table_copy(source, sems, target):
         block = source * 2 + core
@@ -459,12 +530,19 @@
         chain=lambda: remote(
             next_state, before.at[own_heads], state_send.at[3], state_recv.at[3], ep=me + 2
         ),
-        mixed=lambda: remote(
-            mixed.at[partner], mixed_peer, mixed_send.at[0], mixed_recv.at[0], tp=partner
-        ),
-    )
-
-    copies[0].wait()
+    )
+
+    def mixed_copy(n):
+        lanes = pl.ds(pl.multiple_of(n * tile, tile), tile)
+        return remote(
+            mixed.at[partner, :, lanes],
+            mixed_peer.at[:, lanes],
+            mixed_send.at[n],
+            mixed_recv.at[n],
+            tp=partner,
+        )
+
+    loaded("x", "gain", "index", "score")
     x = x_v[...].astype(f32)
     normed = (
         x * lax.rsqrt(jnp.mean(x * x, axis=1, keepdims=True) + EPSILON) * gain_ref[...]
@@ -472,14 +550,14 @@
     for part in range(SPLIT):
         rows[(chip * SPLIT + part) * 2 + core] = normed[part * part_rows : (part + 1) * part_rows]
     score = score_ref[...]
-    weight = ROUTED_SCALE * score / jnp.sum(score, axis=1, keepdims=True)
-    lane = lax.broadcasted_iota(jnp.int32, (length, LANES), 1)
-    table = jnp.zeros((length, LANES), f32)
-    for k in range(score.shape[1]):
-        table = table + jnp.where(lane == index_ref[:, k : k + 1], weight[:, k : k + 1], 0.0)
-    gates[chip * 2 + core] = table.T[:count]
-
-    pl.semaphore_wait(barrier, 2 + has_right.astype(jnp.int32) + has_left.astype(jnp.int32))
+    weight = ROUTED_SCALE * score / jnp.sum(score, axis=0, keepdims=True)
+    expert = lax.broadcasted_iota(jnp.int32, (count, length), 0)
+    table = jnp.zeros((count, length), f32)
+    for k in range(score.shape[0]):
+        table = table + jnp.where(expert == index_ref[k : k + 1, :], weight[k : k + 1, :], 0.0)
+    gates[chip * 2 + core] = table
+
+    pl.semaphore_wait(barrier, chips + 1)
 
     @pl.when(has_right)
     def _():
@@ -493,19 +571,19 @@
         row_copy(chip * SPLIT + part, side_sem, side).start()
     table_copy(chip, table_side, side).start()
 
-    def send_right(arg):
+    def send_right(arg, first):
         row_copy(arg, right_sem, me + 2).start()
 
-    def send_left(arg):
+    def send_left(arg, first):
         row_copy(arg, left_sem, me - 2).start()
 
-    def forward(arg):
-        source, part = arg // SPLIT, arg % SPLIT
+    def forward(arg, first):
+        source = arg // SPLIT
         arrived_row(arg * 2 + core)
         to_right = jnp.logical_and(source < chip, has_right)
         to_left = jnp.logical_and(source > chip, has_left)
 
-        @pl.when(part == 0)
+        @pl.when(first)
         def _():
             arrived_table(source * 2 + core)
 
@@ -521,17 +599,23 @@
 
         @pl.when(to_right)
         def _():
-            send_right(arg)
+            send_right(arg, first)
 
         @pl.when(to_left)
         def _():
-            send_left(arg)
+            send_left(arg, first)
 
         row_copy(arg, side_sem, side).start()
 
-    def mix_local(arg):
-        for i in (1, 2, 3):
-            copies[i].wait()
+    def cross(arg, first):
+        forward(arg, first)
+        cross_copy(arg).start()
+
+    def mix_local(arg, first):
+        @pl.when(arg == 0)
+        def _():
+            loaded("forget", "query", "value", "margin", "extra")
+
         row = lax.broadcasted_iota(jnp.int32, (length, length), 0)
         column = lax.broadcasted_iota(jnp.int32, (length, length), 1)
         upper = row < BLK
@@ -540,14 +624,15 @@
         crossed = jnp.logical_and(jnp.logical_not(upper), left)
         ones = causal.astype(f32).astype(bf16)
         head_lane = lax.broadcasted_iota(jnp.int32, (length, heads), 1)
+        extra_columns = extra_ref[...].T
         middle = BLK // 2 - 1
 
-        def one_head(h, _):
+        def one_head(h):
             lanes = pl.ds(pl.multiple_of(h * HEAD_CHANNELS, HEAD_CHANNELS), HEAD_CHANNELS)
             query = jax.nn.silu(query_v[:, lanes].astype(f32))
             key = margin_ref[:, lanes] * jax.nn.sigmoid(-forget_v[:, lanes].astype(f32))
             extra = jnp.sum(
-                jnp.where(head_lane == h, extra_ref[...], 0.0), axis=1, keepdims=True
+                jnp.where(head_lane == h, extra_columns, 0.0), axis=1, keepdims=True
             )
             decay = jnp.log1p(-key) + extra
             high = decay.astype(bf16)
@@ -573,13 +658,16 @@
             key_state = jnp.where(upper, key_end * second, key_end).astype(bf16)
             own_state[h] = dot_tn(value, key_state).astype(bf16)
             own_decay[pl.ds(h, 1), :] = first * second
-            return 0
-
-        lax.fori_loop(0, heads, one_head, 0)
-        state_copies["state"]().start()
-        state_copies["decay"]().start()
-
-    def mix_state(arg):
+
+        one_head(2 * arg)
+        one_head(2 * arg + 1)
+
+        @pl.when(arg == heads // 2 - 1)
+        def _():
+            state_copies["state"]().start()
+            state_copies["decay"]().start()
+
+    def mix_state(arg, first):
         state_copies["state"]().wait_recv()
         state_copies["decay"]().wait_recv()
 
@@ -608,15 +696,16 @@
             lax.fori_loop(0, mine, one_head, 0)
             state_copies["chain"]().start()
 
-    def mix_finish(arg):
-        copies[12].wait()
-        copies[13].wait()
-
-        @pl.when(has_left)
+    def mix_finish(arg, first):
+        @pl.when(arg == 0)
+        def _():
+            loaded("output_gate", "head_gain")
+
+        @pl.when(jnp.logical_and(arg == 0, has_left))
         def _():
             state_copies["before"]().wait_recv()
 
-        def one_head(h, _):
+        def one_head(h):
             lanes = pl.ds(pl.multiple_of(h * HEAD_CHANNELS, HEAD_CHANNELS), HEAD_CHANNELS)
             state = before[h].astype(f32)
             beside = side_state[h].astype(f32)
@@ -626,174 +715,206 @@
             factor = lax.rsqrt(jnp.mean(out * out, axis=1, keepdims=True) + EPSILON)
             gate = jax.nn.silu(output_gate_v[:, lanes].astype(f32))
             gated[:, lanes] = (out * factor * head_gain_ref[:, lanes] * gate).astype(bf16)
-            return 0
-
-        lax.fori_loop(0, heads, one_head, 0)
-        tile = 512
+
+        one_head(2 * arg)
+        one_head(2 * arg + 1)
+
+    def mix_project(arg, first):
+        @pl.when(arg == 0)
+        def _():
+            loaded("out_weight")
+
         kept = length // 2
-
-        def one_tile(n, _):
-            lanes = pl.ds(pl.multiple_of(n * tile, tile), tile)
-            partial = dot(gated[...], out_weight_v[:, lanes]).astype(bf16)
-            mixed[0, :, lanes] = partial[:kept]
-            mixed[1, :, lanes] = partial[kept:]
-            return 0
-
-        lax.fori_loop(0, out_weight_v.shape[1] // tile, one_tile, 0)
-        state_copies["mixed"]().start()
-
-    def mix_out(arg):
-        state_copies["mixed"]().wait_recv()
+        lanes = pl.ds(pl.multiple_of(arg * tile, tile), tile)
+        partial = dot(gated[...], out_weight_v[:, lanes]).astype(bf16)
+        mixed[0, :, lanes] = partial[:kept]
+        mixed[1, :, lanes] = partial[kept:]
+
+        mixed_copy(arg).start()
+
+    def mix_out(arg, first):
+        for n in range(tiles):
+            mixed_copy(n).wait_recv()
+
         recurrent_ref[...] = (mixed[half].astype(f32) + mixed_peer[...].astype(f32)).astype(bf16)
 
-    def hidden_part(arg):
+    def hidden_part(arg, first):
         shared = arg == routed
-        source, part = arg // SPLIT, arg % SPLIT
+        chunk = arg // GROUP
+        source, place = chunk // COARSE, chunk % COARSE
 
         @pl.when(shared)
         def _():
-            for i in range(4, 12):
-                copies[i].wait()
+            loaded("shared_gate", "shared_up")
+
+        @pl.when(jnp.logical_and(source == chip, first))
+        def _():
+            loaded("gate", "up")
 
         @pl.when(jnp.logical_not(shared))
         def _():
-            arrived_row(arg * 2 + other)
-
-            @pl.when(part == 0)
+            for p in range(GROUP):
+                arrived_row((arg + p) * 2 + other)
+
+            @pl.when(first)
             def _():
                 arrived_table(source * 2 + other)
 
         which = shared.astype(jnp.int32)
-        low = jnp.where(shared, chip * SPLIT * 2 + core, arg * 2)
-        high = jnp.where(shared, chip * SPLIT * 2 + core + 2, arg * 2 + 1)
-        x = jnp.concatenate([rows[low], rows[high]], axis=0)
+        pieces = []
+        for parity in range(2):
+            for p in range(GROUP):
+                own = (chip * SPLIT + parity * GROUP + p) * 2 + core
+                pieces.append(rows[jnp.where(shared, own, (arg + p) * 2 + parity)])
+        x = jnp.concatenate(pieces, axis=0)
         lane = lax.broadcasted_iota(jnp.int32, (length, count), 1)
         block_low = jnp.where(shared, chip * 2 + core, source * 2)
         block_high = jnp.where(shared, chip * 2 + core, source * 2 + 1)
 
-        def own_gate(place):
-            column = jnp.sum(
-                jnp.where(lane == me, gates[place].T, 0.0), axis=1, keepdims=True
-            )
-            return jnp.where(part == 0, column[:part_rows], column[part_rows:])
+        def own_gate(block):
+            column = jnp.sum(jnp.where(lane == me, gates[block].T, 0.0), axis=1, keepdims=True)
+            return jnp.where(place == 0, column[:coarse_rows], column[coarse_rows:])
 
         routed_gate = jnp.concatenate([own_gate(block_low), own_gate(block_high)], axis=0)
         scale = jnp.where(shared, 1.0, routed_gate)
         gate_part = dot(x, gate_w[which])
         up_part = dot(x, up_w[which])
-        own_hidden[arg] = (jax.nn.silu(gate_part) * up_part * scale).astype(bf16)
-        hidden_copy(arg).start()
-
-    def down_part(arg):
+        own_hidden[chunk] = (jax.nn.silu(gate_part) * up_part * scale).astype(bf16)
+        hidden_copy(chunk).start()
+
+    def down_part(arg, first):
         shared = arg == routed
+        chunk = arg // GROUP
         which = shared.astype(jnp.int32)
-        hidden_copy(arg).wait_recv()
-        out = dot(own_hidden[arg], down_w[which, 0]) + dot(peer_hidden[arg], down_w[which, 1])
+
+        @pl.when(shared)
+        def _():
+            loaded("shared_down0", "shared_down1")
+
+        @pl.when(jnp.logical_and(chunk // COARSE == chip, first))
+        def _():
+            loaded("down0", "down1")
+
+        hidden_copy(chunk).wait_recv()
+        out = dot(own_hidden[chunk], down_w[which, 0]) + dot(peer_hidden[chunk], down_w[which, 1])
         out = out.astype(bf16)
-        result[arg, 0] = out[:part_rows]
-        result[arg, 1] = out[part_rows:]
+        result[chunk, 0] = out[:coarse_rows]
+        result[chunk, 1] = out[coarse_rows:]
 
         @pl.when(jnp.logical_not(shared))
         def _():
-            result_copy(arg).start()
-
-    def chip_sum(arg):
-        result_copy(arg).wait_recv()
-        return result[arg, core].astype(f32) + side_result[arg].astype(f32)
-
-    def to_neighbour(arg):
-        source = arg // SPLIT
-        return source > chip, jnp.abs(source - chip) == 1
-
-    def outward_to(arg, place):
+            result_copy(chunk).start()
+
+    def part_slice(arg):
+        return pl.ds(pl.multiple_of(arg % GROUP * part_rows, part_rows), part_rows)
+
+    def chip_sum(arg, awaited):
+        chunk = arg // GROUP
+
+        @pl.when(awaited)
+        def _():
+            result_copy(chunk).wait_recv()
+
+        inside = part_slice(arg)
+        return result[chunk, core, inside].astype(f32) + side_result[chunk, inside].astype(f32)
+
+    def final_copy(arg):
+        slot = chip * SPLIT + arg % SPLIT
+        there = arg // SPLIT * 2 + core
+        return outward_copy(arg, final.at[slot], final_recv.at[slot], there)
+
+    def send_sum(arg, first, direct):
+        target = arg // SPLIT
+        adjacent = jnp.abs(target - chip) == 1
+        total = chip_sum(arg, arg % GROUP == 0)
+        if direct:
+            outward[arg] = total.astype(bf16)
+            final_copy(arg).start()
+            return
+        inner = jnp.logical_and(has_left, has_right)
+        towards = jnp.where(target > chip, me + 2, me - 2)
+        relay = outward_copy(arg, inward.at[arg], inward_recv.at[arg], towards)
+
+        @pl.when(inner)
+        def _():
+            relay.wait_recv()
+            outward[arg] = (total + inward[arg].astype(f32)).astype(bf16)
+
+        @pl.when(jnp.logical_not(inner))
+        def _():
+            outward[arg] = total.astype(bf16)
+
+        @pl.when(adjacent)
+        def _():
+            final_copy(arg).start()
+
+        @pl.when(jnp.logical_not(adjacent))
+        def _():
+            relay.start()
+
+    def finish(arg, first, left_all, right_all):
         part = arg % SPLIT
-        target, sem, to = (
-            (inward_left.at[part], left_recv.at[part], me + 2),
-            (inward.at[arg], inward_recv.at[arg], me + 2),
-            (inward_right.at[part], right_recv.at[part], me - 2),
-            (inward.at[arg], inward_recv.at[arg], me - 2),
-        )[place]
-        return outward_copy(arg, target, sem, to)
-
-    def send_sum(arg):
-        right, adjacent = to_neighbour(arg)
-        inner = jnp.logical_and(has_left, has_right)
-        total = chip_sum(arg)
-
-        @pl.when(inner)
-        def _():
-            outward_to(arg, 1).wait_recv()
-            outward[arg] = (total + inward[arg].astype(f32)).astype(bf16)
-
-        @pl.when(jnp.logical_not(inner))
-        def _():
-            outward[arg] = total.astype(bf16)
-
-        far = jnp.logical_not(adjacent)
-        for place, (direction, distance) in enumerate(
-            (
-                (right, adjacent),
-                (right, far),
-                (jnp.logical_not(right), adjacent),
-                (jnp.logical_not(right), far),
-            )
-        ):
-
-            @pl.when(jnp.logical_and(direction, distance))
+        place = pl.ds(pl.multiple_of(part * part_rows, part_rows), part_rows)
+        shared = result[last, part // GROUP, part_slice(arg)].astype(f32)
+        total = chip_sum(arg, arg % GROUP == 0) + shared
+        for s in range(chips):
+            taken = jnp.abs(chip - s) == 1
+            if left_all:
+                taken = jnp.logical_or(taken, chip > s)
+            if right_all:
+                taken = jnp.logical_or(taken, chip < s)
+            slot = s * SPLIT + part
+
+            @pl.when(taken)
             def _():
-                outward_to(arg, place).start()
-
-    def finish(arg):
-        part = arg % SPLIT
-        total = chip_sum(arg) + result[routed, part].astype(f32)
-        place = pl.ds(pl.multiple_of(part * part_rows, part_rows), part_rows)
-
-        @pl.when(has_left)
-        def _():
-            outward_to(arg, 0).wait_recv()
-
-        @pl.when(has_right)
-        def _():
-            outward_to(arg, 2).wait_recv()
-
-        from_left = jnp.where(has_left, inward_left[part].astype(f32), 0.0)
-        from_right = jnp.where(has_right, inward_right[part].astype(f32), 0.0)
-        expert_ref[place, :] = (total + from_left + from_right).astype(bf16)
+                outward_copy(arg, final.at[slot], final_recv.at[slot], side).wait_recv()
+
+            total = total + jnp.where(taken, final[slot].astype(f32), 0.0)
+        expert_ref[place, :] = total.astype(bf16)
 
     actions = dict(
         SR=send_right,
         SL=send_left,
         RF=forward,
+        RX=cross,
         MA=mix_local,
         ST=mix_state,
         H=hidden_part,
         D=down_part,
-        S=send_sum,
-        FIN=finish,
+        S=functools.partial(send_sum, direct=False),
+        SX=functools.partial(send_sum, direct=True),
+        FIN=functools.partial(finish, left_all=False, right_all=False),
+        FL=functools.partial(finish, left_all=True, right_all=False),
+        FR=functools.partial(finish, left_all=False, right_all=True),
+        FB=functools.partial(finish, left_all=True, right_all=True),
         MB=mix_finish,
+        MP=mix_project,
         MO=mix_out,
     )
     mine_words = []
-    for n in range(steps // 3):
+    for n in range(steps // 2):
         word = jnp.int32(words[0][n])
         for c in range(1, chips):
             word = jnp.where(chip == c, words[c][n], word)
         mine_words.append(word)
 
     def turn(i, _):
-        place, digit = i // 3, i % 3
+        place, digit = i // 2, i % 2
         word = mine_words[0]
-        for n in range(1, steps // 3):
+        for n in range(1, steps // 2):
             word = jnp.where(place == n, mine_words[n], word)
         code = jnp.where(
-            digit == 0, word % 256, jnp.where(digit == 1, word // 256 % 256, word // 65536)
+            digit == 0, word % 32768, word // 32768
         )
-        kind, arg = code // 16, code % 16
+        kind, arg, turned = code // 128, code // 2 % 64, code % 2
+        first = arg % SPLIT == 0
+        shift = (arg % SPLIT + half * (SPLIT // 2)) % SPLIT
+        arg = jnp.where(turned == 1, arg // SPLIT * SPLIT + shift, arg)
         for name, action in actions.items():
 
             @pl.when(kind == NUMBER[name])
             def _():
-                action(arg)
+                action(arg, first)
 
         return 0
 
@@ -801,17 +922,32 @@
 
     def drain(arg, _):
         source, part = arg // SPLIT, arg % SPLIT
-        hidden_copy(arg).wait_send()
-        result_copy(arg).wait_send()
         row_copy(arg, side_sem, side).wait_send()
         to_right = jnp.logical_and(source <= chip, has_right)
         to_left = jnp.logical_and(source >= chip, has_left)
-
-        @pl.when(to_right)
+        row_right, row_left = to_right, to_left
+        if CROSSED:
+            kept = (part + half * (SPLIT // 2)) % SPLIT < SPLIT // 2
+            own = source == chip
+            right_end = jnp.logical_and(own, chip == chips - 2)
+            left_end = jnp.logical_and(own, chip == 1)
+            row_right = jnp.logical_and(to_right, jnp.logical_or(kept, jnp.logical_not(right_end)))
+            row_left = jnp.logical_and(to_left, jnp.logical_or(kept, jnp.logical_not(left_end)))
+            ends = jnp.logical_or(
+                jnp.logical_and(chip == chips - 1, source == chips - 2),
+                jnp.logical_and(chip == 0, source == 1),
+            )
+
+            @pl.when(jnp.logical_and(ends, kept))
+            def _():
+                cross_copy(arg).wait_send()
+
+
+        @pl.when(row_right)
         def _():
             row_copy(arg, right_sem, me + 2).wait_send()
 
-        @pl.when(to_left)
+        @pl.when(row_left)
         def _():
             row_copy(arg, left_sem, me - 2).wait_send()
 
@@ -834,7 +970,14 @@
         return 0
 
     lax.fori_loop(0, routed, drain, 0)
-    hidden_copy(routed).wait_send()
+
+    def drain_chunk(chunk, _):
+        hidden_copy(chunk).wait_send()
+        result_copy(chunk).wait_send()
+        return 0
+
+    lax.fori_loop(0, last, drain_chunk, 0)
+    hidden_copy(last).wait_send()
     state_copies["state"]().wait_send()
     state_copies["decay"]().wait_send()
 
@@ -846,7 +989,8 @@
     def _():
         state_copies["chain"]().wait_send()
 
-    state_copies["mixed"]().wait_send()
+    for n in range(tiles):
+        mixed_copy(n).wait_send()
 
 
 def fused_fits(position_decay_extra, chosen_expert_index, routed_gate_weight):
@@ -887,24 +1031,49 @@
     width, width_out = expert_hidden_state.shape[1], recurrence_out_weight.shape[1]
     units, features = routed_gate_weight.shape[2], routed_down_weight.shape[2]
     part_rows = length // SPLIT
-    hbm = pl.BlockSpec(memory_space=pl.ANY)
+    hbm = pl.BlockSpec(memory_space=pltpu.HBM)
     vmem = pl.BlockSpec(memory_space=pltpu.VMEM)
     dma = pltpu.SemaphoreType.DMA
     mixer_rows = pltpu.VMEM((length, channels), bf16)
-    hidden = pltpu.VMEM((routed + 1, 2 * part_rows, units), bf16)
+    coarse_rows = length // COARSE
+    chunks = chips * COARSE + 1
+    hidden = pltpu.VMEM((chunks, 2 * coarse_rows, units), bf16)
     partial = pltpu.VMEM((routed, part_rows, features), bf16)
-    edge = pltpu.VMEM((SPLIT, part_rows, features), bf16)
     state = pltpu.VMEM((heads, HEAD_CHANNELS, HEAD_CHANNELS), bf16)
     decay = pltpu.VMEM((heads, HEAD_CHANNELS), f32)
+    large = [
+        pltpu.with_memory_space_constraint(array, pltpu.HBM)
+        for array in (
+            recurrence_query_input,
+            forget_gate_input,
+            recurrence_value_input,
+            output_gate_input,
+            recurrence_out_weight,
+            expert_hidden_state,
+            routed_gate_weight,
+            routed_up_weight,
+            routed_down_weight,
+            shared_gate_weight,
+            shared_up_weight,
+            shared_down_weight,
+            forget_lower_margin[None, :],
+            position_decay_extra.T,
+            head_norm_gain[None, :],
+            chosen_expert_index.T,
+            chosen_expert_score.T,
+            expert_norm_gain[None, :],
+        )
+    ]
     return pl.pallas_call(
         functools.partial(fused_kernel, count),
         out_shape=(
             jax.ShapeDtypeStruct((length // 2, width_out), bf16),
             jax.ShapeDtypeStruct((length, features), bf16),
         ),
-        in_specs=[hbm] * 12 + [vmem] * 6,
+        in_specs=[hbm] * 18,
         out_specs=(vmem, vmem),
         scratch_shapes=[
+            *(pltpu.VMEM(array.shape, array.dtype) for array in large[12:]),
             mixer_rows,
             mixer_rows,
             mixer_rows,
@@ -918,11 +1087,10 @@
             pltpu.VMEM((count, count, length), f32),
             hidden,
             hidden,
-            pltpu.VMEM((routed + 1, 2, part_rows, features), bf16),
+            pltpu.VMEM((chunks, 2, coarse_rows, features), bf16),
+            pltpu.VMEM((chunks, coarse_rows, features), bf16),
             partial,
             partial,
-            edge,
-            edge,
             partial,
             pltpu.VMEM((length, channels), f32),
             mixer_rows,
@@ -935,54 +1103,37 @@
             mixer_rows,
             pltpu.VMEM((2, length // 2, width_out), bf16),
             pltpu.VMEM((length // 2, width_out), bf16),
-            dma((14,)),
+            dma((20,)),
             dma((routed * 2,)),
             dma((count,)),
+            dma((routed,)),
             dma((routed,)),
             dma((routed,)),
             dma((routed,)),
             dma((chips,)),
             dma((chips,)),
             dma((chips,)),
-            dma((routed + 1,)),
-            dma((routed + 1,)),
+            dma((chunks,)),
+            dma((chunks,)),
+            dma((chunks,)),
+            dma((chunks,)),
             dma((routed,)),
             dma((routed,)),
             dma((routed,)),
-            dma((routed,)),
-            dma((SPLIT,)),
-            dma((SPLIT,)),
             dma((4,)),
             dma((4,)),
-            dma((1,)),
-            dma((1,)),
+            dma((4,)),
+            dma((4,)),
         ],
         compiler_params=pltpu.CompilerParams(
-            collective_id=0, has_side_effects=True, vmem_limit_bytes=56 * 1024 * 1024
+            collective_id=0, has_side_effects=True, vmem_limit_bytes=46 * 1024 * 1024
         ),
         cost_estimate=pl.CostEstimate(
             flops=9_000_000_000, bytes_accessed=18_000_000, transcendentals=0
         ),
         name="fused_kernel",
     )(
-        recurrence_query_input,
-        forget_gate_input,
-        recurrence_value_input,
-        output_gate_input,
-        recurrence_out_weight,
-        expert_hidden_state,
-        routed_gate_weight,
-        routed_up_weight,
-        routed_down_weight,
-        shared_gate_weight,
-        shared_up_weight,
-        shared_down_weight,
-        forget_lower_margin[None, :],
-        position_decay_extra,
-        head_norm_gain[None, :],
-        chosen_expert_index,
-        chosen_expert_score,
-        expert_norm_gain[None, :],
+        *large,
     )
 
 

time: 76.5 us -> 61.8 us (0.81); the launches traced: 76.2 us -> 60.7 us
  Pallas kernels: 68 us -> 58.7 us
  local copies, waits for them, and re-layouts: 7.59 us -> 1.41 us
    pallas_call x1, Pallas kernels: 68 us -> 58.7 us  [fused_layer(): pl.pallas_call(functools.partial(fused_kernel, count), out_shape=(jax.Sha...]
    unnamed x5 -> x2, local copies, waits for them, and re-layouts: 7.59 us -> 1.41 us
where the time goes in v2:
time: 61.8 us; the launch traced here: 60.7 us
  Pallas kernels  58.7 us (95%)
  local copies, waits for them, and re-layouts  1.41 us (2%)
  between operations  0.65 us (1%)
    pallas_call x1, Pallas kernels, fused_layer(): pl.pallas_call(functools.partial(fused_kernel, count), out_shape=(jax.Sha...  58.7 us
    unnamed x2, local copies, waits for them, and re-layouts  1.41 us

profile of v2, /device:TPU:0, one launch (start us, length us, event | category | flops | bytes accessed | tf_op | source)
XLA Modules:
  0.0 60.7 jit_solution(7004767302209523774)
XLA Ops:
  0.6 58.7 %fused_kernel.1 = (bf16[64,2048]{1,0:T(8,128)(2,1)S(1)}, bf16[128,1024]{1,0:T(8,128)(2,1)S(1)}) custom-call(bf16[128,1024]{1,0:T(8,128)(2,1)} %query_hbm.1, bf16[128,1024]{1,0:T(8,128)(2,1)} %forget_hbm.1, bf16[128,1024]{1,0:T(8,128)(2,1)} %value_hbm.1, bf16[128,1024]{1,0:T(8,128)(2,1)} %output_gate_hbm.1, bf16[1024,2048]{1,0:T(8,128)(2,1)} %out_weight_hbm.1, ...), custom_call_target="tpu_custom_call" | custom-call | flops 8999999488 | bytes 18000000 | tf_op jit(solution)/shard_map/fused_kernel/pallas_call | solution.py:1067
  59.3 0.7 %copy.22 = bf16[64,2048]{1,0:T(8,128)(2,1)} copy(bf16[64,2048]{1,0:T(8,128)(2,1)S(1)} %get-tuple-element.4) | data formatting | bytes 524288
  60.0 0.7 %copy.23 = bf16[128,1024]{1,0:T(8,128)(2,1)} copy(bf16[128,1024]{1,0:T(8,128)(2,1)S(1)} %get-tuple-element.5) | data formatting | bytes 524288

commit v3 on v2

--- a/solution.py
+++ b/solution.py
@@ -191,13 +191,14 @@
 SPLIT = 4
 COARSE = 2
 GROUP = SPLIT // COARSE
-CROSSED = True
+CROSSED = 1
 KINDS = (
     "NO",
     "SR",
     "SL",
     "RF",
     "RX",
+    "RN",
     "MA",
     "ST",
     "H",
@@ -211,72 +212,73 @@
     "MB",
     "MP",
     "MO",
+    "DR",
 )
 NUMBER = {name: place for place, name in enumerate(KINDS)}
 
 
 ORDERS = (
     (
-        ("SR", 0, 1, 0), ("SR", 0, 0, 0), ("SR", 0, 2, 0), ("H", 4, 0, 0), ("MA", 0, 0, 0),
-        ("MA", 0, 1, 0), ("MA", 0, 2, 0), ("MA", 0, 3, 0), ("H", 0, 0, 0), ("H", 0, 2, 0),
-        ("ST", 0, 0, 0), ("SR", 0, 3, 0), ("D", 4, 0, 0), ("MB", 0, 0, 0), ("MB", 0, 1, 0),
-        ("MB", 0, 2, 0), ("RX", 1, 0, 1), ("D", 0, 0, 0), ("RF", 2, 0, 0), ("D", 0, 2, 0),
-        ("RX", 1, 1, 1), ("RF", 1, 2, 1), ("H", 1, 0, 1), ("RF", 2, 1, 0), ("H", 2, 0, 0),
-        ("RF", 1, 3, 1), ("RF", 3, 0, 0), ("H", 1, 2, 1), ("D", 1, 2, 1), ("RF", 3, 1, 0),
-        ("S", 1, 2, 1), ("S", 1, 3, 1), ("H", 3, 0, 0), ("D", 2, 0, 0), ("RF", 3, 2, 0),
-        ("S", 2, 0, 0), ("S", 2, 1, 0), ("RF", 3, 3, 0), ("H", 3, 2, 0), ("D", 3, 0, 0),
-        ("RF", 2, 2, 0), ("S", 3, 0, 0), ("SX", 3, 1, 0), ("RF", 2, 3, 0), ("MB", 0, 3, 0),
-        ("MP", 0, 0, 0), ("MP", 0, 1, 0), ("H", 2, 2, 0), ("D", 3, 2, 0), ("MP", 0, 2, 0),
-        ("MP", 0, 3, 0), ("S", 3, 2, 0), ("S", 3, 3, 0), ("D", 1, 0, 1), ("S", 1, 0, 1),
-        ("S", 1, 1, 1), ("D", 2, 2, 0), ("S", 2, 2, 0), ("S", 2, 3, 0), ("MO", 0, 0, 0),
-        ("FR", 0, 2, 0), ("FIN", 0, 0, 0), ("FR", 0, 3, 0), ("FIN", 0, 1, 0),
+        ("SR", 0, 0, 0), ("SR", 0, 1, 0), ("SR", 0, 3, 0), ("SR", 0, 2, 0), ("H", 4, 0, 0),
+        ("MA", 0, 0, 0), ("H", 0, 0, 0), ("H", 0, 2, 0), ("MA", 0, 1, 0), ("MA", 0, 2, 0),
+        ("MA", 0, 3, 0), ("RX", 1, 0, 1), ("D", 4, 0, 0), ("ST", 0, 0, 0), ("RX", 1, 1, 1),
+        ("D", 0, 0, 0), ("H", 1, 0, 1), ("D", 0, 2, 0), ("RF", 2, 0, 1), ("RF", 1, 2, 1),
+        ("RF", 2, 1, 1), ("H", 2, 0, 1), ("RF", 1, 3, 1), ("RF", 3, 0, 0), ("H", 1, 2, 1),
+        ("D", 1, 2, 1), ("RF", 3, 1, 0), ("S", 1, 2, 1), ("S", 1, 3, 1), ("H", 3, 0, 0),
+        ("RF", 3, 2, 0), ("D", 1, 0, 1), ("RF", 3, 3, 0), ("S", 1, 0, 1), ("S", 1, 1, 1),
+        ("H", 3, 2, 0), ("RF", 2, 2, 1), ("D", 3, 0, 0), ("S", 3, 0, 0), ("S", 3, 1, 0),
+        ("RF", 2, 3, 1), ("H", 2, 2, 1), ("D", 3, 2, 0), ("D", 2, 2, 1), ("S", 3, 2, 0),
+        ("S", 3, 3, 0), ("MB", 0, 0, 0), ("S", 2, 2, 1), ("S", 2, 3, 1), ("MB", 0, 1, 0),
+        ("MB", 0, 2, 0), ("MB", 0, 3, 0), ("MP", 0, 0, 0), ("MP", 0, 1, 0), ("D", 2, 0, 1),
+        ("MP", 0, 2, 0), ("MP", 0, 3, 0), ("S", 2, 0, 1), ("S", 2, 1, 1), ("FIN", 0, 0, 0),
+        ("FIN", 0, 1, 0), ("MO", 0, 0, 0), ("FIN", 0, 2, 0), ("DR", 0, 0, 0), ("FIN", 0, 3, 0),
     ),
     (
-        ("SR", 1, 0, 0), ("SR", 1, 1, 0), ("SR", 1, 2, 0), ("H", 4, 0, 0), ("MA", 0, 0, 0),
-        ("H", 1, 0, 0), ("H", 1, 2, 0), ("SL", 1, 0, 1), ("MA", 0, 1, 0), ("MA", 0, 2, 0),
-        ("MA", 0, 3, 0), ("RF", 2, 0, 0), ("D", 4, 0, 0), ("SL", 1, 1, 1), ("RF", 0, 0, 0),
-        ("RF", 0, 1, 0), ("RF", 2, 1, 0), ("D", 1, 0, 0), ("H", 0, 0, 0), ("H", 2, 0, 0),
-        ("RF", 3, 0, 0), ("D", 1, 2, 0), ("RF", 0, 2, 0), ("RF", 3, 1, 0), ("D", 0, 0, 0),
-        ("RF", 0, 3, 0), ("SR", 1, 3, 0), ("ST", 0, 0, 0), ("H", 3, 0, 0), ("H", 0, 2, 0),
-        ("D", 2, 0, 0), ("MB", 0, 0, 0), ("RF", 3, 2, 0), ("MB", 0, 1, 0), ("MB", 0, 2, 0),
-        ("RF", 3, 3, 0), ("MB", 0, 3, 0), ("MP", 0, 0, 0), ("MP", 0, 1, 0), ("H", 3, 2, 0),
-        ("D", 3, 0, 0), ("RF", 2, 2, 0), ("MP", 0, 2, 0), ("MP", 0, 3, 0), ("D", 0, 2, 0),
-        ("RF", 2, 3, 0), ("SX", 0, 2, 0), ("SX", 0, 3, 0), ("H", 2, 2, 0), ("D", 3, 2, 0),
-        ("S", 2, 0, 0), ("S", 2, 1, 0), ("MO", 0, 0, 0), ("S", 3, 0, 0), ("D", 2, 2, 0),
-        ("SX", 3, 1, 0), ("S", 3, 2, 0), ("S", 0, 0, 0), ("S", 3, 3, 0), ("S", 0, 1, 0),
-        ("S", 2, 2, 0), ("S", 2, 3, 0), ("FIN", 1, 2, 1), ("FIN", 1, 0, 1), ("FIN", 1, 1, 1),
-        ("FIN", 1, 3, 1),
+        ("SR", 1, 0, 1), ("SR", 1, 1, 1), ("SL", 1, 0, 1), ("SL", 1, 1, 1), ("H", 4, 0, 0),
+        ("MA", 0, 0, 0), ("MA", 0, 1, 0), ("MA", 0, 2, 0), ("H", 1, 0, 0), ("H", 1, 2, 0),
+        ("RF", 0, 0, 0), ("RF", 2, 0, 1), ("RF", 0, 1, 0), ("H", 0, 0, 0), ("RF", 2, 1, 1),
+        ("D", 1, 0, 0), ("H", 2, 0, 1), ("RF", 3, 0, 0), ("RF", 0, 2, 0), ("D", 1, 2, 0),
+        ("RF", 0, 3, 0), ("SR", 1, 2, 1), ("SR", 1, 3, 1), ("RF", 3, 1, 0), ("H", 0, 2, 0),
+        ("D", 0, 0, 0), ("H", 3, 0, 0), ("RF", 3, 2, 0), ("MA", 0, 3, 0), ("RF", 3, 3, 0),
+        ("ST", 0, 0, 0), ("D", 0, 2, 0), ("H", 3, 2, 0), ("MB", 0, 0, 0), ("RF", 2, 2, 1),
+        ("MB", 0, 1, 0), ("MB", 0, 2, 0), ("MB", 0, 3, 0), ("D", 3, 0, 0), ("MP", 0, 0, 0),
+        ("MP", 0, 1, 0), ("RF", 2, 3, 1), ("MP", 0, 2, 0), ("MP", 0, 3, 0), ("H", 2, 2, 1),
+        ("D", 3, 2, 0), ("D", 2, 2, 1), ("MO", 0, 0, 0), ("S", 3, 0, 0), ("S", 3, 1, 0),
+        ("D", 2, 0, 1), ("S", 3, 2, 0), ("S", 0, 0, 0), ("S", 3, 3, 0), ("S", 0, 1, 0),
+        ("S", 2, 2, 1), ("S", 0, 2, 0), ("S", 2, 3, 1), ("D", 4, 0, 0), ("S", 0, 3, 0),
+        ("S", 2, 0, 1), ("FIN", 1, 2, 1), ("S", 2, 1, 1), ("FIN", 1, 3, 1), ("FIN", 1, 0, 1),
+        ("DR", 0, 0, 0), ("FIN", 1, 1, 1),
     ),
     (
-        ("H", 4, 0, 0), ("SL", 2, 0, 0), ("SL", 2, 1, 0), ("SR", 2, 1, 1), ("MA", 0, 0, 0),
-        ("H", 2, 0, 0), ("H", 2, 2, 0), ("MA", 0, 1, 0), ("MA", 0, 2, 0), ("RF", 1, 0, 0),
-        ("SR", 2, 0, 1), ("RF", 3, 0, 0), ("MA", 0, 3, 0), ("D", 4, 0, 0), ("RF", 1, 1, 0),
-        ("D", 2, 0, 0), ("H", 1, 0, 0), ("RF", 3, 1, 0), ("D", 2, 2, 0), ("H", 3, 0, 0),
-        ("RF", 0, 0, 0), ("RF", 3, 2, 0), ("RF", 3, 3, 0), ("SL", 2, 2, 0), ("SL", 2, 3, 0),
-        ("H", 3, 2, 0), ("D", 1, 0, 0), ("RF", 0, 1, 0), ("RF", 1, 2, 0), ("D", 3, 0, 0),
-        ("H", 0, 0, 0), ("RF", 0, 2, 0), ("D", 3, 2, 0), ("RF", 0, 3, 0), ("H", 0, 2, 0),
-        ("RF", 1, 3, 0), ("D", 0, 0, 0), ("H", 1, 2, 0), ("ST", 0, 0, 0), ("MB", 0, 0, 0),
-        ("MB", 0, 1, 0), ("MB", 0, 2, 0), ("MB", 0, 3, 0), ("D", 0, 2, 0), ("MP", 0, 0, 0),
-        ("MP", 0, 1, 0), ("MP", 0, 2, 0), ("MP", 0, 3, 0), ("SX", 0, 2, 0), ("SX", 0, 3, 0),
-        ("D", 1, 2, 0), ("S", 1, 0, 0), ("S", 1, 1, 0), ("S", 0, 0, 0), ("MO", 0, 0, 0),
-        ("S", 0, 1, 0), ("S", 3, 0, 0), ("SX", 3, 1, 0), ("S", 3, 2, 0), ("S", 3, 3, 0),
-        ("S", 1, 2, 0), ("S", 1, 3, 0), ("FIN", 2, 2, 1), ("FIN", 2, 3, 1), ("FIN", 2, 0, 1),
-        ("FIN", 2, 1, 1),
+        ("SR", 2, 1, 1), ("SR", 2, 0, 1), ("SL", 2, 0, 1), ("SL", 2, 1, 1), ("H", 4, 0, 0),
+        ("MA", 0, 0, 0), ("H", 2, 0, 0), ("H", 2, 2, 0), ("RF", 1, 0, 1), ("MA", 0, 1, 0),
+        ("MA", 0, 2, 0), ("RF", 3, 0, 0), ("MA", 0, 3, 0), ("D", 4, 0, 0), ("RF", 1, 1, 1),
+        ("RF", 3, 1, 0), ("H", 1, 0, 1), ("D", 2, 0, 0), ("RF", 0, 0, 0), ("RF", 3, 2, 0),
+        ("D", 2, 2, 0), ("RF", 0, 1, 0), ("RF", 3, 3, 0), ("SL", 2, 2, 1), ("SL", 2, 3, 1),
+        ("H", 0, 0, 0), ("RF", 0, 2, 0), ("RF", 0, 3, 0), ("D", 0, 0, 0), ("H", 0, 2, 0),
+        ("RF", 1, 2, 1), ("H", 3, 0, 0), ("RF", 1, 3, 1), ("H", 1, 2, 1), ("D", 1, 2, 1),
+        ("D", 0, 2, 0), ("ST", 0, 0, 0), ("D", 3, 0, 0), ("MB", 0, 0, 0), ("MB", 0, 1, 0),
+        ("MB", 0, 2, 0), ("MB", 0, 3, 0), ("MP", 0, 0, 0), ("H", 3, 2, 0), ("D", 1, 0, 1),
+        ("MP", 0, 1, 0), ("MP", 0, 2, 0), ("MP", 0, 3, 0), ("S", 0, 0, 0), ("S", 0, 1, 0),
+        ("S", 3, 0, 0), ("S", 0, 2, 0), ("S", 3, 1, 0), ("D", 3, 2, 0), ("S", 0, 3, 0),
+        ("S", 1, 2, 1), ("S", 3, 2, 0), ("S", 1, 3, 1), ("MO", 0, 0, 0), ("S", 3, 3, 0),
+        ("S", 1, 0, 1), ("FIN", 2, 2, 1), ("S", 1, 1, 1), ("FIN", 2, 3, 1), ("FIN", 2, 0, 1),
+        ("DR", 0, 0, 0), ("FIN", 2, 1, 1),
     ),
     (
-        ("SL", 3, 0, 0), ("SL", 3, 3, 0), ("SL", 3, 1, 0), ("SL", 3, 2, 0), ("H", 4, 0, 0),
+        ("SL", 3, 0, 0), ("SL", 3, 1, 0), ("SL", 3, 2, 0), ("H", 4, 0, 0), ("SL", 3, 3, 0),
         ("MA", 0, 0, 0), ("MA", 0, 1, 0), ("H", 3, 0, 0), ("H", 3, 2, 0), ("MA", 0, 2, 0),
-        ("MA", 0, 3, 0), ("D", 4, 0, 0), ("D", 3, 0, 0), ("RF", 1, 0, 0), ("D", 3, 2, 0),
-        ("RX", 2, 0, 1), ("RX", 2, 1, 1), ("RF", 1, 1, 0), ("H", 2, 0, 1), ("H", 1, 0, 0),
+        ("MA", 0, 3, 0), ("D", 4, 0, 0), ("RX", 2, 0, 1), ("RX", 2, 1, 1), ("H", 2, 0, 1),
+        ("RF", 1, 0, 1), ("D", 3, 0, 0), ("D", 3, 2, 0), ("RF", 1, 1, 1), ("H", 1, 0, 1),
         ("RF", 2, 2, 1), ("RF", 0, 0, 0), ("RF", 2, 3, 1), ("RF", 0, 1, 0), ("H", 2, 2, 1),
-        ("H", 0, 0, 0), ("D", 2, 2, 1), ("RF", 1, 2, 0), ("S", 2, 2, 1), ("S", 2, 3, 1),
-        ("D", 1, 0, 0), ("RF", 0, 2, 0), ("S", 1, 0, 0), ("S", 1, 1, 0), ("D", 2, 0, 1),
-        ("RF", 0, 3, 0), ("S", 2, 0, 1), ("S", 2, 1, 1), ("H", 0, 2, 0), ("D", 0, 0, 0),
-        ("RF", 1, 3, 0), ("S", 0, 0, 0), ("S", 0, 1, 0), ("H", 1, 2, 0), ("ST", 0, 0, 0),
-        ("MB", 0, 0, 0), ("D", 0, 2, 0), ("MB", 0, 1, 0), ("MB", 0, 2, 0), ("MB", 0, 3, 0),
-        ("MP", 0, 0, 0), ("SX", 0, 2, 0), ("SX", 0, 3, 0), ("MP", 0, 1, 0), ("MP", 0, 2, 0),
-        ("MP", 0, 3, 0), ("D", 1, 2, 0), ("S", 1, 2, 0), ("S", 1, 3, 0), ("FIN", 3, 0, 0),
-        ("FL", 3, 1, 0), ("MO", 0, 0, 0), ("FIN", 3, 2, 0), ("FIN", 3, 3, 0),
+        ("H", 0, 0, 0), ("D", 2, 2, 1), ("RF", 0, 2, 0), ("S", 2, 2, 1), ("S", 2, 3, 1),
+        ("RF", 0, 3, 0), ("H", 0, 2, 0), ("D", 2, 0, 1), ("RF", 1, 2, 1), ("S", 2, 0, 1),
+        ("D", 0, 0, 0), ("S", 2, 1, 1), ("RF", 1, 3, 1), ("S", 0, 0, 0), ("S", 0, 1, 0),
+        ("H", 1, 2, 1), ("D", 0, 2, 0), ("D", 1, 2, 1), ("ST", 0, 0, 0), ("S", 0, 2, 0),
+        ("S", 0, 3, 0), ("S", 1, 2, 1), ("S", 1, 3, 1), ("MB", 0, 0, 0), ("MB", 0, 1, 0),
+        ("MB", 0, 2, 0), ("MB", 0, 3, 0), ("MP", 0, 0, 0), ("MP", 0, 1, 0), ("D", 1, 0, 1),
+        ("MP", 0, 2, 0), ("MP", 0, 3, 0), ("S", 1, 0, 1), ("S", 1, 1, 1), ("FIN", 3, 0, 0),
+        ("FIN", 3, 1, 0), ("MO", 0, 0, 0), ("FIN", 3, 2, 0), ("DR", 0, 0, 0), ("FIN", 3, 3, 0),
     ),
 )
 
@@ -443,19 +445,34 @@
         name: pltpu.make_async_copy(source, target, load_sem.at[i])
         for i, (name, (source, target)) in enumerate(loads.items())
     }
-    for copy in copies.values():
-        copy.start()
+    early = ("x", "gain", "index", "score")
+    for name in early:
+        copies[name].start()
+
+    barrier = pltpu.get_barrier_semaphore()
+    pl.semaphore_signal(barrier, inc=1, device_id={"ep": side}, device_id_type=MESH)
+    pl.semaphore_signal(barrier, inc=1, device_id={"tp": partner}, device_id_type=MESH)
+
+    def greet(there):
+        pl.semaphore_signal(barrier, inc=1, device_id={"ep": there}, device_id_type=MESH)
+
+    greeted = 2
+    if any(kind == "SX" for order in chip_orders(chips) for kind, *_ in order):
+        for distance in range(1, chips):
+            greet((chip + distance) % chips * 2 + core)
+        greeted = greeted + chips - 1
+    else:
+        pl.when(has_right)(functools.partial(greet, me + 2))
+        pl.when(has_left)(functools.partial(greet, me - 2))
+        greeted = greeted + has_right.astype(jnp.int32) + has_left.astype(jnp.int32)
+
+    for name in copies:
+        if name not in early:
+            copies[name].start()
 
     def loaded(*names):
         for name in names:
             copies[name].wait()
-
-    barrier = pltpu.get_barrier_semaphore()
-    pl.semaphore_signal(barrier, inc=1, device_id={"ep": side}, device_id_type=MESH)
-    pl.semaphore_signal(barrier, inc=1, device_id={"tp": partner}, device_id_type=MESH)
-    for distance in range(1, chips):
-        there = (chip + distance) % chips * 2 + core
-        pl.semaphore_signal(barrier, inc=1, device_id={"ep": there}, device_id_type=MESH)
 
     def remote(source, target, send, recv, **device):
         return pltpu.make_async_remote_copy(
@@ -542,13 +559,14 @@
             tp=partner,
         )
 
-    loaded("x", "gain", "index", "score")
+    loaded("x", "gain")
     x = x_v[...].astype(f32)
     normed = (
         x * lax.rsqrt(jnp.mean(x * x, axis=1, keepdims=True) + EPSILON) * gain_ref[...]
     ).astype(bf16)
     for part in range(SPLIT):
         rows[(chip * SPLIT + part) * 2 + core] = normed[part * part_rows : (part + 1) * part_rows]
+    loaded("index", "score")
     score = score_ref[...]
     weight = ROUTED_SCALE * score / jnp.sum(score, axis=0, keepdims=True)
     expert = lax.broadcasted_iota(jnp.int32, (count, length), 0)
@@ -557,7 +575,7 @@
         table = table + jnp.where(expert == index_ref[k : k + 1, :], weight[k : k + 1, :], 0.0)
     gates[chip * 2 + core] = table
 
-    pl.semaphore_wait(barrier, chips + 1)
+    pl.semaphore_wait(barrier, greeted)
 
     @pl.when(has_right)
     def _():
@@ -577,7 +595,7 @@
     def send_left(arg, first):
         row_copy(arg, left_sem, me - 2).start()
 
-    def forward(arg, first):
+    def forward(arg, first, onward=True):
         source = arg // SPLIT
         arrived_row(arg * 2 + core)
         to_right = jnp.logical_and(source < chip, has_right)
@@ -597,13 +615,15 @@
 
             table_copy(source, table_side, side).start()
 
-        @pl.when(to_right)
-        def _():
-            send_right(arg, first)
-
-        @pl.when(to_left)
-        def _():
-            send_left(arg, first)
+        if onward:
+
+            @pl.when(to_right)
+            def _():
+                send_right(arg, first)
+
+            @pl.when(to_left)
+            def _():
+                send_left(arg, first)
 
         row_copy(arg, side_sem, side).start()
 
@@ -872,11 +892,91 @@
             total = total + jnp.where(taken, final[slot].astype(f32), 0.0)
         expert_ref[place, :] = total.astype(bf16)
 
+    def drain_all(_, first):
+        def drain(arg, _):
+            source, part = arg // SPLIT, arg % SPLIT
+            row_copy(arg, side_sem, side).wait_send()
+            to_right = jnp.logical_and(source <= chip, has_right)
+            to_left = jnp.logical_and(source >= chip, has_left)
+            row_right, row_left = to_right, to_left
+            if CROSSED:
+                inner = jnp.logical_and(source > 0, source < chips - 1)
+                kept = (part + half * (SPLIT // 2)) % SPLIT < SPLIT // 2
+
+                def crosses(end):
+                    if CROSSED == 2:
+                        return inner
+                    return jnp.logical_and(inner, jnp.abs(source - end) == 1)
+
+                held = jnp.logical_not(kept)
+                to_last = jnp.logical_and(chip == chips - 2, crosses(chips - 1))
+                to_first = jnp.logical_and(chip == 1, crosses(0))
+                row_right = jnp.logical_and(to_right, jnp.logical_not(jnp.logical_and(held, to_last)))
+                row_left = jnp.logical_and(to_left, jnp.logical_not(jnp.logical_and(held, to_first)))
+                ends = jnp.logical_or(
+                    jnp.logical_and(chip == chips - 1, crosses(chips - 1)),
+                    jnp.logical_and(chip == 0, crosses(0)),
+                )
+
+                @pl.when(jnp.logical_and(ends, kept))
+                def _():
+                    cross_copy(arg).wait_send()
+
+            @pl.when(row_right)
+            def _():
+                row_copy(arg, right_sem, me + 2).wait_send()
+
+            @pl.when(row_left)
+            def _():
+                row_copy(arg, left_sem, me - 2).wait_send()
+
+            @pl.when(source != chip)
+            def _():
+                outward_copy(arg, inward.at[arg], inward_recv.at[arg], side).wait_send()
+
+            @pl.when(part == 0)
+            def _():
+                table_copy(source, table_side, side).wait_send()
+
+                @pl.when(to_right)
+                def _():
+                    table_copy(source, table_right, me + 2).wait_send()
+
+                @pl.when(to_left)
+                def _():
+                    table_copy(source, table_left, me - 2).wait_send()
+
+            return 0
+
+        lax.fori_loop(0, routed, drain, 0)
+
+        def drain_chunk(chunk, _):
+            hidden_copy(chunk).wait_send()
+            result_copy(chunk).wait_send()
+            return 0
+
+        lax.fori_loop(0, last, drain_chunk, 0)
+        hidden_copy(last).wait_send()
+        state_copies["state"]().wait_send()
+        state_copies["decay"]().wait_send()
+
+        @pl.when(has_left)
+        def _():
+            state_copies["before"]().wait_send()
+
+        @pl.when(has_right)
+        def _():
+            state_copies["chain"]().wait_send()
+
+        for n in range(tiles):
+            mixed_copy(n).wait_send()
+
     actions = dict(
         SR=send_right,
         SL=send_left,
         RF=forward,
         RX=cross,
+        RN=functools.partial(forward, onward=False),
         MA=mix_local,
         ST=mix_state,
         H=hidden_part,
@@ -890,6 +990,7 @@
         MB=mix_finish,
         MP=mix_project,
         MO=mix_out,
+        DR=drain_all,
     )
     mine_words = []
     for n in range(steps // 2):
@@ -919,78 +1020,6 @@
         return 0
 
     lax.fori_loop(0, steps, turn, 0)
-
-    def drain(arg, _):
-        source, part = arg // SPLIT, arg % SPLIT
-        row_copy(arg, side_sem, side).wait_send()
-        to_right = jnp.logical_and(source <= chip, has_right)
-        to_left = jnp.logical_and(source >= chip, has_left)
-        row_right, row_left = to_right, to_left
-        if CROSSED:
-            kept = (part + half * (SPLIT // 2)) % SPLIT < SPLIT // 2
-            own = source == chip
-            right_end = jnp.logical_and(own, chip == chips - 2)
-            left_end = jnp.logical_and(own, chip == 1)
-            row_right = jnp.logical_and(to_right, jnp.logical_or(kept, jnp.logical_not(right_end)))
-            row_left = jnp.logical_and(to_left, jnp.logical_or(kept, jnp.logical_not(left_end)))
-            ends = jnp.logical_or(
-                jnp.logical_and(chip == chips - 1, source == chips - 2),
-                jnp.logical_and(chip == 0, source == 1),
-            )
-
-            @pl.when(jnp.logical_and(ends, kept))
-            def _():
-                cross_copy(arg).wait_send()
-
-
-        @pl.when(row_right)
-        def _():
-            row_copy(arg, right_sem, me + 2).wait_send()
-
-        @pl.when(row_left)
-        def _():
-            row_copy(arg, left_sem, me - 2).wait_send()
-
-        @pl.when(source != chip)
-        def _():
-            outward_copy(arg, inward.at[arg], inward_recv.at[arg], side).wait_send()
-
-        @pl.when(part == 0)
-        def _():
-            table_copy(source, table_side, side).wait_send()
-
-            @pl.when(to_right)
-            def _():
-                table_copy(source, table_right, me + 2).wait_send()
-
-            @pl.when(to_left)
-            def _():
-                table_copy(source, table_left, me - 2).wait_send()
-
-        return 0
-
-    lax.fori_loop(0, routed, drain, 0)
-
-    def drain_chunk(chunk, _):
-        hidden_copy(chunk).wait_send()
-        result_copy(chunk).wait_send()
-        return 0
-
-    lax.fori_loop(0, last, drain_chunk, 0)
-    hidden_copy(last).wait_send()
-    state_copies["state"]().wait_send()
-    state_copies["decay"]().wait_send()
-
-    @pl.when(has_left)
-    def _():
-        state_copies["before"]().wait_send()
-
-    @pl.when(has_right)
-    def _():
-        state_copies["chain"]().wait_send()
-
-    for n in range(tiles):
-        mixed_copy(n).wait_send()
 
 
 def fused_fits(position_decay_extra, chosen_expert_index, routed_gate_weight):

time: 61.8 us -> 59 us (0.955); the launches traced: 60.7 us -> 58.9 us
  Pallas kernels: 58.7 us -> 56.8 us
    pallas_call x1, Pallas kernels: 58.7 us -> 56.8 us  [fused_layer(): pl.pallas_call(functools.partial(fused_kernel, count), out_shape=(jax.Sha...]
where the time goes in v3:
time: 59 us; the launch traced here: 58.9 us
  Pallas kernels  56.8 us (96%)
  local copies, waits for them, and re-layouts  1.41 us (2%)
  between operations  0.65 us (1%)
    pallas_call x1, Pallas kernels, fused_layer(): pl.pallas_call(functools.partial(fused_kernel, count), out_shape=(jax.Sha...  56.8 us
    unnamed x2, local copies, waits for them, and re-layouts  1.41 us

profile of v3, /device:TPU:0, one launch (start us, length us, event | category | flops | bytes accessed | tf_op | source)
XLA Modules:
  0.0 58.9 jit_solution(2401955887595369838)
XLA Ops:
  0.6 56.8 %fused_kernel.1 = (bf16[64,2048]{1,0:T(8,128)(2,1)S(1)}, bf16[128,1024]{1,0:T(8,128)(2,1)S(1)}) custom-call(bf16[128,1024]{1,0:T(8,128)(2,1)} %query_hbm.1, bf16[128,1024]{1,0:T(8,128)(2,1)} %forget_hbm.1, bf16[128,1024]{1,0:T(8,128)(2,1)} %value_hbm.1, bf16[128,1024]{1,0:T(8,128)(2,1)} %output_gate_hbm.1, bf16[1024,2048]{1,0:T(8,128)(2,1)} %out_weight_hbm.1, ...), custom_call_target="tpu_custom_call" | custom-call | flops 8999999488 | bytes 18000000 | tf_op jit(solution)/shard_map/fused_kernel/pallas_call | solution.py:1096
  57.5 0.7 %copy.22 = bf16[64,2048]{1,0:T(8,128)(2,1)} copy(bf16[64,2048]{1,0:T(8,128)(2,1)S(1)} %get-tuple-element.4) | data formatting | bytes 524288
  58.2 0.7 %copy.23 = bf16[128,1024]{1,0:T(8,128)(2,1)} copy(bf16[128,1024]{1,0:T(8,128)(2,1)S(1)} %get-tuple-element.5) | data formatting | bytes 524288

commit v4 on v3

--- a/solution.py
+++ b/solution.py
@@ -219,67 +219,72 @@
 
 ORDERS = (
     (
-        ("SR", 0, 0, 0), ("SR", 0, 1, 0), ("SR", 0, 3, 0), ("SR", 0, 2, 0), ("H", 4, 0, 0),
-        ("MA", 0, 0, 0), ("H", 0, 0, 0), ("H", 0, 2, 0), ("MA", 0, 1, 0), ("MA", 0, 2, 0),
-        ("MA", 0, 3, 0), ("RX", 1, 0, 1), ("D", 4, 0, 0), ("ST", 0, 0, 0), ("RX", 1, 1, 1),
-        ("D", 0, 0, 0), ("H", 1, 0, 1), ("D", 0, 2, 0), ("RF", 2, 0, 1), ("RF", 1, 2, 1),
-        ("RF", 2, 1, 1), ("H", 2, 0, 1), ("RF", 1, 3, 1), ("RF", 3, 0, 0), ("H", 1, 2, 1),
-        ("D", 1, 2, 1), ("RF", 3, 1, 0), ("S", 1, 2, 1), ("S", 1, 3, 1), ("H", 3, 0, 0),
-        ("RF", 3, 2, 0), ("D", 1, 0, 1), ("RF", 3, 3, 0), ("S", 1, 0, 1), ("S", 1, 1, 1),
-        ("H", 3, 2, 0), ("RF", 2, 2, 1), ("D", 3, 0, 0), ("S", 3, 0, 0), ("S", 3, 1, 0),
-        ("RF", 2, 3, 1), ("H", 2, 2, 1), ("D", 3, 2, 0), ("D", 2, 2, 1), ("S", 3, 2, 0),
-        ("S", 3, 3, 0), ("MB", 0, 0, 0), ("S", 2, 2, 1), ("S", 2, 3, 1), ("MB", 0, 1, 0),
-        ("MB", 0, 2, 0), ("MB", 0, 3, 0), ("MP", 0, 0, 0), ("MP", 0, 1, 0), ("D", 2, 0, 1),
-        ("MP", 0, 2, 0), ("MP", 0, 3, 0), ("S", 2, 0, 1), ("S", 2, 1, 1), ("FIN", 0, 0, 0),
-        ("FIN", 0, 1, 0), ("MO", 0, 0, 0), ("FIN", 0, 2, 0), ("DR", 0, 0, 0), ("FIN", 0, 3, 0),
+        ("SR", 0, 1, 0), ("SR", 0, 2, 0), ("SR", 0, 3, 0), ("H", 4, 0, 0), ("MA", 0, 0, 0),
+        ("H", 0, 0, 0), ("MA", 0, 1, 0), ("MA", 0, 2, 0), ("H", 0, 2, 0), ("MA", 0, 3, 0),
+        ("D", 4, 0, 0), ("ST", 0, 0, 0), ("MB", 0, 0, 0), ("RX", 1, 0, 1), ("MB", 0, 1, 0),
+        ("D", 0, 0, 0), ("MB", 0, 2, 0), ("RX", 1, 1, 1), ("D", 0, 2, 0), ("H", 1, 0, 1),
+        ("RF", 2, 0, 1), ("RF", 1, 2, 1), ("RF", 2, 1, 1), ("H", 2, 0, 1), ("RF", 1, 3, 1),
+        ("RF", 3, 0, 0), ("H", 1, 2, 1), ("D", 1, 2, 1), ("RF", 3, 1, 0), ("S", 1, 2, 1),
+        ("S", 1, 3, 1), ("MB", 0, 3, 0), ("H", 3, 0, 0), ("RF", 3, 2, 0), ("MP", 0, 0, 0),
+        ("D", 1, 0, 1), ("RF", 3, 3, 0), ("S", 1, 0, 1), ("S", 1, 1, 1), ("H", 3, 2, 0),
+        ("RF", 2, 2, 1), ("D", 3, 0, 0), ("S", 3, 0, 0), ("S", 3, 1, 0), ("RF", 2, 3, 1),
+        ("H", 2, 2, 1), ("D", 3, 2, 0), ("D", 2, 2, 1), ("S", 3, 2, 0), ("S", 3, 3, 0),
+        ("S", 2, 2, 1), ("S", 2, 3, 1), ("MP", 0, 1, 0), ("MP", 0, 2, 0), ("MP", 0, 3, 0),
+        ("D", 2, 0, 1), ("S", 2, 0, 1), ("S", 2, 1, 1), ("FIN", 0, 0, 0), ("MO", 0, 0, 0),
+        ("FIN", 0, 1, 0), ("FIN", 0, 2, 0), ("DR", 0, 0, 0), ("FIN", 0, 3, 0),
     ),
     (
-        ("SR", 1, 0, 1), ("SR", 1, 1, 1), ("SL", 1, 0, 1), ("SL", 1, 1, 1), ("H", 4, 0, 0),
-        ("MA", 0, 0, 0), ("MA", 0, 1, 0), ("MA", 0, 2, 0), ("H", 1, 0, 0), ("H", 1, 2, 0),
-        ("RF", 0, 0, 0), ("RF", 2, 0, 1), ("RF", 0, 1, 0), ("H", 0, 0, 0), ("RF", 2, 1, 1),
-        ("D", 1, 0, 0), ("H", 2, 0, 1), ("RF", 3, 0, 0), ("RF", 0, 2, 0), ("D", 1, 2, 0),
-        ("RF", 0, 3, 0), ("SR", 1, 2, 1), ("SR", 1, 3, 1), ("RF", 3, 1, 0), ("H", 0, 2, 0),
-        ("D", 0, 0, 0), ("H", 3, 0, 0), ("RF", 3, 2, 0), ("MA", 0, 3, 0), ("RF", 3, 3, 0),
-        ("ST", 0, 0, 0), ("D", 0, 2, 0), ("H", 3, 2, 0), ("MB", 0, 0, 0), ("RF", 2, 2, 1),
-        ("MB", 0, 1, 0), ("MB", 0, 2, 0), ("MB", 0, 3, 0), ("D", 3, 0, 0), ("MP", 0, 0, 0),
-        ("MP", 0, 1, 0), ("RF", 2, 3, 1), ("MP", 0, 2, 0), ("MP", 0, 3, 0), ("H", 2, 2, 1),
-        ("D", 3, 2, 0), ("D", 2, 2, 1), ("MO", 0, 0, 0), ("S", 3, 0, 0), ("S", 3, 1, 0),
-        ("D", 2, 0, 1), ("S", 3, 2, 0), ("S", 0, 0, 0), ("S", 3, 3, 0), ("S", 0, 1, 0),
-        ("S", 2, 2, 1), ("S", 0, 2, 0), ("S", 2, 3, 1), ("D", 4, 0, 0), ("S", 0, 3, 0),
-        ("S", 2, 0, 1), ("FIN", 1, 2, 1), ("S", 2, 1, 1), ("FIN", 1, 3, 1), ("FIN", 1, 0, 1),
-        ("DR", 0, 0, 0), ("FIN", 1, 1, 1),
+        ("SL", 1, 1, 1), ("SL", 1, 0, 1), ("H", 4, 0, 0), ("SR", 1, 1, 1), ("MA", 0, 0, 0),
+        ("MA", 0, 1, 0), ("MA", 0, 2, 0), ("H", 1, 0, 0), ("H", 1, 2, 0), ("RF", 0, 0, 0),
+        ("MA", 0, 3, 0), ("RF", 2, 0, 1), ("D", 4, 0, 0), ("RF", 0, 1, 0), ("RF", 2, 1, 1),
+        ("H", 0, 0, 0), ("D", 1, 0, 0), ("RF", 0, 2, 0), ("H", 2, 0, 1), ("RF", 3, 0, 0),
+        ("RF", 0, 3, 0), ("SR", 1, 2, 1), ("D", 1, 2, 0), ("SR", 1, 3, 1), ("H", 0, 2, 0),
+        ("RF", 3, 1, 0), ("ST", 0, 0, 0), ("D", 0, 0, 0), ("H", 3, 0, 0), ("MB", 0, 0, 0),
+        ("RF", 3, 2, 0), ("MB", 0, 1, 0), ("MB", 0, 2, 0), ("MB", 0, 3, 0), ("MP", 0, 0, 0),
+        ("MP", 0, 1, 0), ("MP", 0, 2, 0), ("RF", 3, 3, 0), ("MP", 0, 3, 0), ("D", 0, 2, 0),
+        ("H", 3, 2, 0), ("RF", 2, 2, 1), ("D", 3, 0, 0), ("RF", 2, 3, 1), ("H", 2, 2, 1),
+        ("D", 2, 2, 1), ("MO", 0, 0, 0), ("D", 3, 2, 0), ("S", 3, 0, 0), ("D", 2, 0, 1),
+        ("S", 3, 1, 0), ("S", 0, 0, 0), ("S", 3, 2, 0), ("S", 0, 1, 0), ("S", 3, 3, 0),
+        ("S", 2, 2, 1), ("S", 0, 2, 0), ("S", 2, 3, 1), ("S", 0, 3, 0), ("S", 2, 0, 1),
+        ("FIN", 1, 2, 1), ("S", 2, 1, 1), ("FIN", 1, 3, 1), ("FIN", 1, 0, 1), ("DR", 0, 0, 0),
+        ("FIN", 1, 1, 1),
     ),
     (
-        ("SR", 2, 1, 1), ("SR", 2, 0, 1), ("SL", 2, 0, 1), ("SL", 2, 1, 1), ("H", 4, 0, 0),
-        ("MA", 0, 0, 0), ("H", 2, 0, 0), ("H", 2, 2, 0), ("RF", 1, 0, 1), ("MA", 0, 1, 0),
-        ("MA", 0, 2, 0), ("RF", 3, 0, 0), ("MA", 0, 3, 0), ("D", 4, 0, 0), ("RF", 1, 1, 1),
-        ("RF", 3, 1, 0), ("H", 1, 0, 1), ("D", 2, 0, 0), ("RF", 0, 0, 0), ("RF", 3, 2, 0),
-        ("D", 2, 2, 0), ("RF", 0, 1, 0), ("RF", 3, 3, 0), ("SL", 2, 2, 1), ("SL", 2, 3, 1),
-        ("H", 0, 0, 0), ("RF", 0, 2, 0), ("RF", 0, 3, 0), ("D", 0, 0, 0), ("H", 0, 2, 0),
-        ("RF", 1, 2, 1), ("H", 3, 0, 0), ("RF", 1, 3, 1), ("H", 1, 2, 1), ("D", 1, 2, 1),
-        ("D", 0, 2, 0), ("ST", 0, 0, 0), ("D", 3, 0, 0), ("MB", 0, 0, 0), ("MB", 0, 1, 0),
-        ("MB", 0, 2, 0), ("MB", 0, 3, 0), ("MP", 0, 0, 0), ("H", 3, 2, 0), ("D", 1, 0, 1),
-        ("MP", 0, 1, 0), ("MP", 0, 2, 0), ("MP", 0, 3, 0), ("S", 0, 0, 0), ("S", 0, 1, 0),
-        ("S", 3, 0, 0), ("S", 0, 2, 0), ("S", 3, 1, 0), ("D", 3, 2, 0), ("S", 0, 3, 0),
-        ("S", 1, 2, 1), ("S", 3, 2, 0), ("S", 1, 3, 1), ("MO", 0, 0, 0), ("S", 3, 3, 0),
-        ("S", 1, 0, 1), ("FIN", 2, 2, 1), ("S", 1, 1, 1), ("FIN", 2, 3, 1), ("FIN", 2, 0, 1),
-        ("DR", 0, 0, 0), ("FIN", 2, 1, 1),
+        ("SL", 2, 1, 1), ("SR", 2, 1, 1), ("H", 4, 0, 0), ("MA", 0, 0, 0), ("H", 2, 0, 0),
+        ("H", 2, 2, 0), ("RF", 1, 0, 1), ("MA", 0, 1, 0), ("MA", 0, 2, 0), ("RF", 3, 0, 0),
+        ("MA", 0, 3, 0), ("D", 4, 0, 0), ("RF", 1, 1, 1), ("RF", 3, 1, 0), ("H", 1, 0, 1),
+        ("H", 3, 0, 0), ("RF", 0, 0, 0), ("RF", 3, 2, 0), ("D", 2, 0, 0), ("D", 2, 2, 0),
+        ("RF", 0, 1, 0), ("RF", 3, 3, 0), ("SL", 2, 2, 1), ("SL", 2, 3, 1), ("H", 0, 0, 0),
+        ("RF", 0, 2, 0), ("H", 3, 2, 0), ("D", 3, 0, 0), ("RF", 0, 3, 0), ("H", 0, 2, 0),
+        ("RF", 1, 2, 1), ("D", 0, 0, 0), ("D", 3, 2, 0), ("RF", 1, 3, 1), ("H", 1, 2, 1),
+        ("ST", 0, 0, 0), ("D", 0, 2, 0), ("D", 1, 2, 1), ("MB", 0, 0, 0), ("MB", 0, 1, 0),
+        ("MB", 0, 2, 0), ("MB", 0, 3, 0), ("MP", 0, 0, 0), ("MP", 0, 1, 0), ("MP", 0, 2, 0),
+        ("MP", 0, 3, 0), ("D", 1, 0, 1), ("S", 0, 0, 0), ("S", 0, 1, 0), ("S", 3, 0, 0),
+        ("S", 0, 2, 0), ("MO", 0, 0, 0), ("S", 3, 1, 0), ("S", 0, 3, 0), ("S", 1, 2, 1),
+        ("S", 1, 3, 1), ("S", 3, 2, 0), ("S", 1, 0, 1), ("S", 3, 3, 0), ("S", 1, 1, 1),
+        ("FIN", 2, 2, 1), ("FIN", 2, 3, 1), ("FIN", 2, 0, 1), ("DR", 0, 0, 0), ("FIN", 2, 1, 1),
     ),
     (
-        ("SL", 3, 0, 0), ("SL", 3, 1, 0), ("SL", 3, 2, 0), ("H", 4, 0, 0), ("SL", 3, 3, 0),
-        ("MA", 0, 0, 0), ("MA", 0, 1, 0), ("H", 3, 0, 0), ("H", 3, 2, 0), ("MA", 0, 2, 0),
-        ("MA", 0, 3, 0), ("D", 4, 0, 0), ("RX", 2, 0, 1), ("RX", 2, 1, 1), ("H", 2, 0, 1),
-        ("RF", 1, 0, 1), ("D", 3, 0, 0), ("D", 3, 2, 0), ("RF", 1, 1, 1), ("H", 1, 0, 1),
-        ("RF", 2, 2, 1), ("RF", 0, 0, 0), ("RF", 2, 3, 1), ("RF", 0, 1, 0), ("H", 2, 2, 1),
-        ("H", 0, 0, 0), ("D", 2, 2, 1), ("RF", 0, 2, 0), ("S", 2, 2, 1), ("S", 2, 3, 1),
-        ("RF", 0, 3, 0), ("H", 0, 2, 0), ("D", 2, 0, 1), ("RF", 1, 2, 1), ("S", 2, 0, 1),
-        ("D", 0, 0, 0), ("S", 2, 1, 1), ("RF", 1, 3, 1), ("S", 0, 0, 0), ("S", 0, 1, 0),
-        ("H", 1, 2, 1), ("D", 0, 2, 0), ("D", 1, 2, 1), ("ST", 0, 0, 0), ("S", 0, 2, 0),
-        ("S", 0, 3, 0), ("S", 1, 2, 1), ("S", 1, 3, 1), ("MB", 0, 0, 0), ("MB", 0, 1, 0),
-        ("MB", 0, 2, 0), ("MB", 0, 3, 0), ("MP", 0, 0, 0), ("MP", 0, 1, 0), ("D", 1, 0, 1),
-        ("MP", 0, 2, 0), ("MP", 0, 3, 0), ("S", 1, 0, 1), ("S", 1, 1, 1), ("FIN", 3, 0, 0),
-        ("FIN", 3, 1, 0), ("MO", 0, 0, 0), ("FIN", 3, 2, 0), ("DR", 0, 0, 0), ("FIN", 3, 3, 0),
+        ("SL", 3, 1, 0), ("H", 4, 0, 0), ("MA", 0, 0, 0), ("H", 3, 0, 0), ("MA", 0, 1, 0),
+        ("MA", 0, 2, 0), ("MA", 0, 3, 0), ("RX", 2, 0, 1), ("SL", 3, 2, 0), ("SL", 3, 3, 0),
+        ("D", 4, 0, 0), ("RX", 2, 1, 1), ("H", 2, 0, 1), ("D", 3, 0, 0), ("RF", 1, 0, 1),
+        ("RF", 2, 2, 1), ("RF", 2, 3, 1), ("RF", 0, 0, 0), ("H", 2, 2, 1), ("RF", 1, 1, 1),
+        ("D", 2, 2, 1), ("H", 1, 0, 1), ("RF", 0, 1, 0), ("S", 2, 2, 1), ("S", 2, 3, 1),
+        ("H", 0, 0, 0), ("RF", 0, 2, 0), ("D", 2, 0, 1), ("RF", 0, 3, 0), ("S", 2, 0, 1),
+        ("S", 2, 1, 1), ("H", 0, 2, 0), ("RF", 1, 2, 1), ("D", 0, 0, 0), ("H", 3, 2, 0),
+        ("RF", 1, 3, 1), ("S", 0, 0, 0), ("S", 0, 1, 0), ("H", 1, 2, 1), ("D", 0, 2, 0),
+        ("ST", 0, 0, 0), ("D", 1, 2, 1), ("S", 0, 2, 0), ("S", 0, 3, 0), ("MB", 0, 0, 0),
+        ("MB", 0, 1, 0), ("S", 1, 2, 1), ("S", 1, 3, 1), ("MB", 0, 2, 0), ("MB", 0, 3, 0),
+        ("MP", 0, 0, 0), ("MP", 0, 1, 0), ("D", 1, 0, 1), ("MP", 0, 2, 0), ("MP", 0, 3, 0),
+        ("D", 3, 2, 0), ("S", 1, 0, 1), ("S", 1, 1, 1), ("FIN", 3, 0, 0), ("FIN", 3, 1, 0),
+        ("MO", 0, 0, 0), ("FIN", 3, 2, 0), ("DR", 0, 0, 0), ("FIN", 3, 3, 0),
     ),
+)
+HEADS = (
+    (1, 0, 0),
+    (1, 0, 0),
+    (1, 1, 0),
+    (0, 1, 0),
 )
 
 
@@ -560,12 +565,38 @@
         )
 
     loaded("x", "gain")
-    x = x_v[...].astype(f32)
-    normed = (
-        x * lax.rsqrt(jnp.mean(x * x, axis=1, keepdims=True) + EPSILON) * gain_ref[...]
-    ).astype(bf16)
+
+    def norm_rows(part):
+        x = x_v[pl.ds(pl.multiple_of(part * part_rows, part_rows), part_rows), :].astype(f32)
+        scale = lax.rsqrt(jnp.mean(x * x, axis=1, keepdims=True) + EPSILON)
+        rows[(chip * SPLIT + part) * 2 + core] = (x * scale * gain_ref[...]).astype(bf16)
+
+    def of_chip(column):
+        value = jnp.int32(HEADS[0][column])
+        for c in range(1, chips):
+            value = jnp.where(chip == c, HEADS[c][column], value)
+        return value
+
+    opening = of_chip(2)
+    if CROSSED:
+        middle_chip = jnp.logical_and(has_left, has_right)
+        shifted = (opening + half * (SPLIT // 2)) % SPLIT
+        opening = jnp.where(middle_chip, shifted, opening)
+    norm_rows(opening)
+    pl.semaphore_wait(barrier, greeted)
+
+    @pl.when(of_chip(0) == 1)
+    def _():
+        row_copy(chip * SPLIT + opening, right_sem, me + 2).start()
+
+    @pl.when(of_chip(1) == 1)
+    def _():
+        row_copy(chip * SPLIT + opening, left_sem, me - 2).start()
+
+    for part in range(1, SPLIT):
+        norm_rows((opening + part) % SPLIT)
     for part in range(SPLIT):
-        rows[(chip * SPLIT + part) * 2 + core] = normed[part * part_rows : (part + 1) * part_rows]
+        row_copy(chip * SPLIT + part, side_sem, side).start()
     loaded("index", "score")
     score = score_ref[...]
     weight = ROUTED_SCALE * score / jnp.sum(score, axis=0, keepdims=True)
@@ -575,8 +606,6 @@
         table = table + jnp.where(expert == index_ref[k : k + 1, :], weight[k : k + 1, :], 0.0)
     gates[chip * 2 + core] = table
 
-    pl.semaphore_wait(barrier, greeted)
-
     @pl.when(has_right)
     def _():
         table_copy(chip, table_right, me + 2).start()
@@ -585,8 +614,6 @@
     def _():
         table_copy(chip, table_left, me - 2).start()
 
-    for part in range(SPLIT):
-        row_copy(chip * SPLIT + part, side_sem, side).start()
     table_copy(chip, table_side, side).start()
 
     def send_right(arg, first):

time: 59 us -> 58.5 us (level)
  no operation moved by 1% of the time
where the time goes in v4:
time: 58.5 us; the launch traced here: 58.4 us
  Pallas kernels  56.3 us (96%)
  local copies, waits for them, and re-layouts  1.41 us (2%)
  between operations  0.65 us (1%)
    pallas_call x1, Pallas kernels, fused_layer(): pl.pallas_call(functools.partial(fused_kernel, count), out_shape=(jax.Sha...  56.3 us
    unnamed x2, local copies, waits for them, and re-layouts  1.41 us

profile of v4, /device:TPU:0, one launch (start us, length us, event | category | flops | bytes accessed | tf_op | source)
XLA Modules:
  0.0 58.4 jit_solution(18030281050260410860)
XLA Ops:
  0.6 56.3 %fused_kernel.1 = (bf16[64,2048]{1,0:T(8,128)(2,1)S(1)}, bf16[128,1024]{1,0:T(8,128)(2,1)S(1)}) custom-call(bf16[128,1024]{1,0:T(8,128)(2,1)} %query_hbm.1, bf16[128,1024]{1,0:T(8,128)(2,1)} %forget_hbm.1, bf16[128,1024]{1,0:T(8,128)(2,1)} %value_hbm.1, bf16[128,1024]{1,0:T(8,128)(2,1)} %output_gate_hbm.1, bf16[1024,2048]{1,0:T(8,128)(2,1)} %out_weight_hbm.1, ...), custom_call_target="tpu_custom_call" | custom-call | flops 8999999488 | bytes 18000000 | tf_op jit(solution)/shard_map/fused_kernel/pallas_call | solution.py:1123
  57.0 0.7 %copy.22 = bf16[64,2048]{1,0:T(8,128)(2,1)} copy(bf16[64,2048]{1,0:T(8,128)(2,1)S(1)} %get-tuple-element.4) | data formatting | bytes 524288
  57.7 0.7 %copy.23 = bf16[128,1024]{1,0:T(8,128)(2,1)} copy(bf16[128,1024]{1,0:T(8,128)(2,1)S(1)} %get-tuple-element.5) | data formatting | bytes 524288
